TPU v7x, 32 devices: a whole 2x2x4 slice. The times are simulated.
32 devices in a mesh: grp: 2 (over x), ep: 4 (over y, core), tp: 4 (over z).
Axes of the slice: x: 2, y: 2, z: 4, core: 2. Of those that a mesh axis runs over, the one named last changes fastest.
Arguments:
- mixer_in: bfloat16 [4096, 2048], P(('grp', 'ep', 'tp')), parts along dimension 0, may hold values from -600 to 600
- mixer_gain: float32 [2048], replicated, may hold values from 0.1 to 1.9
- w_query: bfloat16 [2048, 1024], P(None, 'tp'), may hold values from -6 to 6
- w_key: bfloat16 [2048, 512], P(None, 'tp'), may hold values from -0.1875 to 0.1875
- w_value: bfloat16 [2048, 512], P(None, 'tp'), may hold values from -0.25 to 0.25
- sink_logit: float32 [16], P('tp'), may hold values from 3 to 9
- moe_in: bfloat16 [4096, 2048], P(('grp', 'ep', 'tp')), parts along dimension 0, may hold values from -600 to 600
- moe_gain: float32 [2048], replicated, may hold values from 0.1 to 1.9
- router: bfloat16 [2048, 16], replicated, may hold values from -0.25 to 0.25
- routes: int32 [4096, 4], P(('grp', 'ep', 'tp')), parts along dimension 0, may hold values from 0 to 15, all different within a row; in each aligned block of 128 rows (0 to 127, 128 to 255, ...) at most 48 rows name the same one
- expert_gate: bfloat16 [16, 2048, 512], P(('ep', 'tp')), may hold values from -0.125 to 0.125
- expert_up: bfloat16 [16, 2048, 512], P(('ep', 'tp')), may hold values from -0.125 to 0.125
- expert_down: bfloat16 [16, 512, 2048], P(('ep', 'tp')), may hold values from -0.25 to 0.25
- shared_gate: bfloat16 [2048, 512], P(None, 'tp'), may hold values from -0.125 to 0.125
- shared_up: bfloat16 [2048, 512], P(None, 'tp'), may hold values from -0.125 to 0.125
- shared_down: bfloat16 [512, 2048], P('tp'), may hold values from -0.25 to 0.25
Outputs:
- mixed: bfloat16 [4096, 1024], P(('grp', 'ep'), 'tp'), parts along dimension 0
- moe_out: bfloat16 [4096, 2048], P(('grp', 'ep', 'tp')), parts along dimension 0
There are 2 independent parts, one for each index of `grp`. A program takes and returns all parts, laid end to end along the dimension named above; an argument that names none is the same for every part. Nothing has to cross between parts.
Inputs may be any that keep to these rules, and one draw needn't show every extreme that they name: `routes`: each row names 4 different experts. Within the rows of one device (aligned blocks of 128 rows) no expert is named by more than 48 rows, a bound that some block reaches.
All inputs are finite; a program needn't handle non-finite values.
Results may differ from a plain program's by a relative error of at most 0.012.
Values may be sent and summed in bfloat16 or wider, within the bound.
A program may use at most 128 MiB of HBM per device.

v0:
```python
import jax
import jax.numpy as jnp
from jax import lax
from jax.sharding import PartitionSpec as P

HEAD_DIM = 64
WINDOW = 128


EPS = 1e-06
THETA = 10000.0
ROUTED_SCALE = 2.5


def extended(block, sides, width):
    for axis, dim in sides:
        count = lax.axis_size(axis)
        forward = [(i, i + 1) for i in range(count - 1)]
        backward = [(target, source) for source, target in forward]
        low = lax.ppermute(
            lax.slice_in_dim(block, block.shape[dim] - width, None, axis=dim), axis, forward
        )
        high = lax.ppermute(lax.slice_in_dim(block, 0, width, axis=dim), axis, backward)
        block = jnp.concatenate([low, block, high], axis=dim)
    return block


def rms_rows(row_block, gain_vector):
    values = row_block.astype(jnp.float32)
    factor = lax.rsqrt(jnp.mean(values * values, axis=-1, keepdims=True) + EPS)
    return (values * factor * gain_vector).astype(jnp.bfloat16)


def rotate(head_rows, positions):
    half_width = head_rows.shape[-1] // 2
    inverse = THETA ** (-(jnp.arange(half_width, dtype=jnp.float32) * 2.0) / head_rows.shape[-1])
    angles = positions.astype(jnp.float32)[:, None] * inverse[None, :]
    cosine_table = jnp.cos(angles)[:, None, :]
    sine_table = jnp.sin(angles)[:, None, :]
    first_half = head_rows[..., :half_width]
    second_half = head_rows[..., half_width:]
    return jnp.concatenate(
        [
            first_half * cosine_table - second_half * sine_table,
            second_half * cosine_table + first_half * sine_table,
        ],
        axis=-1,
    )


def attend(query_rows, stacked, sink_logit, offset, seq_length):
    span_rows, head_count, head_width = query_rows.shape
    kv_local = stacked.shape[1] // (2 * head_width)
    group_size = head_count // kv_local
    key_table = stacked[:, : kv_local * head_width].reshape(-1, kv_local, head_width)
    value_table = stacked[:, kv_local * head_width :].reshape(-1, kv_local, head_width)
    block_rows = 512
    grouped = query_rows.reshape(span_rows, kv_local, group_size, head_width)
    row_ids = jnp.arange(block_rows, dtype=jnp.int32)[:, None]
    col_ids = jnp.arange(block_rows + 2 * WINDOW, dtype=jnp.int32)[None, :]
    sink_table = sink_logit.reshape(kv_local, group_size)[:, :, None, None]

    def one_block(block_index):
        block_start = block_index * block_rows
        query_block = lax.dynamic_slice_in_dim(grouped, block_start, block_rows, 0)
        key_block = lax.dynamic_slice_in_dim(key_table, block_start, block_rows + 2 * WINDOW, 0)
        value_block = lax.dynamic_slice_in_dim(value_table, block_start, block_rows + 2 * WINDOW, 0)
        scores = jnp.einsum(
            "qkgd,ckd->kgqc", query_block, key_block, preferred_element_type=jnp.float32
        ) * head_width ** (-0.5)
        key_pos = offset + block_start - WINDOW + col_ids
        query_pos = offset + block_start + row_ids
        in_window = (
            (jnp.abs(key_pos - query_pos) <= WINDOW) & (key_pos >= 0) & (key_pos < seq_length)
        )
        scores = jnp.where(in_window[None, None], scores, -jnp.inf)
        row_max = jnp.maximum(jnp.max(scores, axis=-1, keepdims=True), sink_table)
        weights = jnp.exp(scores - row_max)
        denominator = jnp.sum(weights, axis=-1, keepdims=True) + jnp.exp(sink_table - row_max)
        probability = (weights / denominator).astype(jnp.bfloat16)
        output = jnp.einsum(
            "kgqc,ckd->qkgd", probability, value_block, preferred_element_type=jnp.float32
        )
        return output.reshape(block_rows, head_count * head_width).astype(jnp.bfloat16)

    blocks_out = lax.map(one_block, jnp.arange(span_rows // block_rows, dtype=jnp.int32))
    return blocks_out.reshape(span_rows, head_count * head_width)


def body(
    mixer_in,
    mixer_gain,
    w_query,
    w_key,
    w_value,
    sink_logit,
    moe_in,
    moe_gain,
    router,
    routes,
    expert_gate,
    expert_up,
    expert_down,
    shared_gate,
    shared_up,
    shared_down,
):
    normed_first = rms_rows(mixer_in, mixer_gain)
    normed_second = rms_rows(moe_in, moe_gain)
    query_cols = w_query.shape[1]
    key_cols = w_key.shape[1]
    joined = jnp.concatenate([w_query, w_key, w_value], axis=1)
    gathered_first, gathered_second = (
        lax.all_gather(normed_first, "tp", axis=0, tiled=True),
        lax.all_gather(normed_second, "tp", axis=0, tiled=True),
    )
    projected = jnp.dot(gathered_first, joined, preferred_element_type=jnp.float32)
    row_block = gathered_second
    hidden = (
        jax.nn.silu(jnp.dot(row_block, shared_gate, preferred_element_type=jnp.float32))
        * jnp.dot(row_block, shared_up, preferred_element_type=jnp.float32)
    ).astype(jnp.bfloat16)
    shared = lax.psum_scatter(
        jnp.dot(hidden, shared_down, preferred_element_type=jnp.float32),
        "tp",
        scatter_dimension=0,
        tiled=True,
    )
    span_rows = projected.shape[0]
    offset = lax.axis_index("ep") * span_rows
    seq_length = span_rows * lax.axis_size("ep")
    positions = offset + jnp.arange(span_rows, dtype=jnp.int32)
    query_rows = rotate(
        projected[:, :query_cols].reshape(span_rows, -1, HEAD_DIM), positions
    ).astype(jnp.bfloat16)
    key_rows = rotate(
        projected[:, query_cols : query_cols + key_cols].reshape(span_rows, -1, HEAD_DIM), positions
    ).astype(jnp.bfloat16)
    value_rows = projected[:, query_cols + key_cols :].astype(jnp.bfloat16)
    stacked = jnp.concatenate([key_rows.reshape(span_rows, key_cols), value_rows], axis=1)
    padded = extended(stacked, (("ep", 0),), WINDOW)
    mixed = attend(query_rows, padded, sink_logit, offset, seq_length)
    tokens = normed_second.shape[0]
    top_count = routes.shape[1]
    experts = router.shape[1]
    capacity = 3 * top_count * tokens // (2 * experts)
    affinity = jax.nn.sigmoid(jnp.dot(normed_second, router, preferred_element_type=jnp.float32))
    hit_table = routes[:, :, None] == jnp.arange(experts, dtype=jnp.int32)[None, None, :]
    chosen = jnp.sum(jnp.where(hit_table, affinity[:, None, :], 0.0), axis=-1)
    route_weight = ROUTED_SCALE * chosen / jnp.sum(chosen, axis=-1, keepdims=True)
    flat_hits = hit_table.reshape(tokens * top_count, experts).astype(jnp.int32)
    slot_index = jnp.sum((jnp.cumsum(flat_hits, axis=0) - 1) * flat_hits, axis=-1)
    target = routes.reshape(-1) * capacity + slot_index
    source = jnp.arange(tokens * top_count, dtype=jnp.int32) // top_count
    outgoing = (
        jnp.zeros((experts * capacity, normed_second.shape[1]), jnp.bfloat16)
        .at[target]
        .set(normed_second[source])
    )
    outgoing = outgoing.reshape(experts, capacity, -1)
    row_block = lax.all_to_all(outgoing, ("ep", "tp"), split_axis=0, concat_axis=0, tiled=True)
    row_shape = row_block.shape
    flat_rows = row_block.reshape(-1, row_shape[-1])
    hidden_rows = (
        jax.nn.silu(jnp.dot(flat_rows, expert_gate[0], preferred_element_type=jnp.float32))
        * jnp.dot(flat_rows, expert_up[0], preferred_element_type=jnp.float32)
    ).astype(jnp.bfloat16)
    returned = lax.all_to_all(
        jnp.dot(hidden_rows, expert_down[0], preferred_element_type=jnp.float32)
        .astype(jnp.bfloat16)
        .reshape(row_shape),
        ("ep", "tp"),
        split_axis=0,
        concat_axis=0,
        tiled=True,
    )
    picked = returned.reshape(experts * capacity, -1)[target].reshape(tokens, top_count, -1)
    routed = jnp.sum(picked.astype(jnp.float32) * route_weight[:, :, None], axis=1)
    moe_out = (routed + shared).astype(jnp.bfloat16)
    return (mixed, moe_out)


def solution(mesh):
    return jax.shard_map(
        body,
        mesh=mesh,
        in_specs=(
            P(("grp", "ep", "tp"), None),
            P(),
            P(None, "tp"),
            P(None, "tp"),
            P(None, "tp"),
            P("tp"),
            P(("grp", "ep", "tp"), None),
            P(),
            P(),
            P(("grp", "ep", "tp"), None),
            P(("ep", "tp"), None, None),
            P(("ep", "tp"), None, None),
            P(("ep", "tp"), None, None),
            P(None, "tp"),
            P(None, "tp"),
            P("tp", None),
        ),
        out_specs=(P(("grp", "ep"), "tp"), P(("grp", "ep", "tp"), None)),
        check_vma=False,
    )
```

profile of v0, /device:TPU:1, one launch (start us, length us, event | category | flops | bytes accessed | tf_op | source)
XLA Modules:
  0.0 331.1 jit_solution(11312634323357929496)
XLA Ops:
  7.2 0.0 copy-start
  7.2 0.0 copy-start.5
  7.2 0.0 all-gather.5.cloned.1.call-start
  7.2 1.4 fusion.30
  8.6 2.0 fusion.32
  10.7 0.0 all-gather.5.cloned.1.call-update
  10.7 0.0 copy-done.5
  10.7 0.1 copy.32
  10.8 0.1 eq.36
  10.9 0.1 eq.32
  11.0 1.2 reduce-window.6
  12.2 0.2 slice_reduce_fusion
  12.5 0.1 copy.31
  12.6 0.1 mul.218
  12.7 0.1 fusion.46
  12.8 12.1 %scatter_custom_fusion = bf16[768,2048]{1,0:T(8,128)(2,1)} fusion(s32[512]{0:T(512)S(1)} %bitcast.87, bf16[128,2048]{1,0:T(8,128)(2,1)} %fusion.32, s32[1024]{0:T(1024)S(1)} %pad_clamp_fusion.1, bf16[]{:T(256)} %constant.88.clone.1), kind=kCustom, calls=%fused_computation.22 | custom fusion | bytes 3146240 | tf_op jit(solution)/shard_map/scatter | solution.py:158
  24.9 0.0 copy-start.2
  24.9 0.0 copy-start.6
  24.9 7.5 %all-to-all-start = ((bf16[16,48,2048]{2,1,0:T(8,128)(2,1)}), bf16[16,48,2048]{2,1,0:T(8,128)(2,1)}, u32[]{:S(2)}, u32[]{:S(2)}) async-start(bf16[16,48,2048]{2,1,0:T(8,128)(2,1)} %bitcast.76), calls=%async_computation | async-start | bytes 6291456 | tf_op jit(solution)/shard_map/all_to_all | solution.py:161
  32.4 0.0 copy-start.3
  32.4 0.0 all-gather.3.cloned.1.call-start
  32.4 0.0 copy-done.2
  32.5 0.2 fusion.27
  32.6 0.0 copy-done.6
  32.7 1.0 fusion.29
  33.6 0.0 all-gather.3.cloned.1.call-update
  33.7 0.2 reduce-scatter.2.cloned.1.call-start
  33.9 60.4 %all-gather.5.cloned.1.call-done = bf16[512,2048]{1,0:T(8,128)(2,1)} async-done(((bf16[128,2048]{1,0:T(8,128)(2,1)}), bf16[512,2048]{1,0:T(8,128)(2,1)}) %all-gather.5.cloned.1.call-update) | async-done | bytes 2097168 | tf_op jit(solution)/shard_map/all_gather | solution.py:115
  94.3 0.0 copy-done.3
  94.3 2.3 fusion.58
  96.6 6.1 %fusion.23 = f32[512,2048]{1,0:T(8,128)} fusion(bf16[128,2048]{1,0:T(8,128)(2,1)} %param.31, bf16[512,2048]{1,0:T(8,128)(2,1)} %all-gather.5.cloned.1.call-done, bf16[2048,128]{1,0:T(8,128)(2,1)} %param.30, f32[512,128]{1,0:T(8,128)S(1)} %fusion.58), kind=kOutput, calls=%fused_computation.36 | convolution fusion | flops 537264128 | bytes 7602176 | tf_op jit(solution)/shard_map/dot_general | solution.py:124
  102.7 0.0 reduce-scatter.2.cloned.1.call-update
  102.7 56.2 %all-to-all-done = bf16[16,48,2048]{2,1,0:T(8,128)(2,1)} async-done(((bf16[16,48,2048]{2,1,0:T(8,128)(2,1)}), bf16[16,48,2048]{2,1,0:T(8,128)(2,1)}, u32[]{:S(2)}, u32[]{:S(2)}) %all-to-all-start) | async-done | bytes 3145760 | tf_op jit(solution)/shard_map/all_to_all | solution.py:161
  158.9 5.5 %fusion.12 = f32[768,512]{1,0:T(8,128)} fusion(bf16[768,2048]{1,0:T(8,128)(2,1)} %bitcast.19, bf16[1,2048,512]{2,1,0:T(8,128)(2,1)} %param.26), kind=kOutput, calls=%fused_computation.20 | convolution fusion | flops 1610612736 | bytes 6815744 | tf_op jit(solution)/shard_map/dot_general | solution.py:165
  164.5 0.0 copy-done
  164.5 8.5 %convolution_convert_fusion = bf16[768,2048]{1,0:T(8,128)(2,1)} fusion(bf16[1,512,2048]{2,1,0:T(8,128)(2,1)S(1)} %copy-done, f32[768,512]{1,0:T(8,128)} %fusion.12, bf16[768,2048]{1,0:T(8,128)(2,1)} %bitcast.19, bf16[1,2048,512]{2,1,0:T(8,128)(2,1)} %param.27), kind=kOutput, calls=%fused_computation.9 | convolution fusion | flops 3225157632 | bytes 12058624 | tf_op jit(solution)/shard_map/dot_general | solution.py:169
  173.0 5.9 %all-to-all-start.1 = ((bf16[16,48,2048]{2,1,0:T(8,128)(2,1)}), bf16[16,48,2048]{2,1,0:T(8,128)(2,1)}, u32[]{:S(2)}, u32[]{:S(2)}) async-start(bf16[16,48,2048]{2,1,0:T(8,128)(2,1)} %bitcast.77), calls=%async_computation.1 | async-start | bytes 6291456 | tf_op jit(solution)/shard_map/all_to_all | solution.py:168
  178.8 0.0 copy-done.7
  178.8 0.1 max.22
  178.9 0.0 copy-done.1
  178.9 0.0 copy-done.4
  178.9 0.2 fusion.26
  179.2 0.1 copy.35
  179.4 0.3 multiply_cosine_fusion
  179.7 0.8 fusion.18
  180.5 0.0 all-gather.3.cloned.1.call-done
  180.5 3.5 %fusion.3 = f32[512,512]{0,1:T(8,128)S(1)} fusion(bf16[512,2048]{1,0:T(8,128)(2,1)} %all-gather.3.cloned.1.call-done, bf16[2048,128]{1,0:T(8,128)(2,1)} %param.20, bf16[2048,128]{1,0:T(8,128)(2,1)} %param.19, bf16[2048,256]{1,0:T(8,128)(2,1)} %param.18), kind=kOutput, calls=%fused_computation.11 | convolution fusion | flops 1080033280 | bytes 5242880 | tf_op jit(solution)/shard_map/dot_general | solution.py:117
  184.3 3.6 %collective-permute-start = (bf16[128,256]{0,1:T(8,128)(2,1)S(1)}, bf16[128,256]{0,1:T(8,128)(2,1)S(1)}, u32[]{:S(2)}, u32[]{:S(2)}) collective-permute-start(bf16[128,256]{0,1:T(8,128)(2,1)S(1)} %get-tuple-element.43), channel_id=1, source_target_pairs={{0,4},{4,8},{8,12},{1,5},{5,9},{9,13},{2,6},{6,10},{10,14},{3,7},{... | collective-permute-start | bytes 196616 | tf_op jit(solution)/shard_map/ppermute | solution.py:20
  187.9 2.1 collective-permute-start.1
  190.0 0.1 subtract_convert_fusion
  190.1 1.5 collective-permute-done
  191.6 2.4 collective-permute-done.1
  194.1 1.3 fusion.1
  195.4 0.1 broadcast_maximum_fusion
  195.4 1.4 fusion
  196.8 0.1 exponential_add_fusion
  196.9 2.0 fusion.21
  198.9 0.8 copy.36
  199.7 105.0 %all-to-all-done.1 = bf16[16,48,2048]{2,1,0:T(8,128)(2,1)} async-done(((bf16[16,48,2048]{2,1,0:T(8,128)(2,1)}), bf16[16,48,2048]{2,1,0:T(8,128)(2,1)}, u32[]{:S(2)}, u32[]{:S(2)}) %all-to-all-start.1) | async-done | bytes 3145760 | tf_op jit(solution)/shard_map/all_to_all | solution.py:168
  304.8 7.5 %gather_fusion = bf16[512,2048]{1,0:T(8,128)(2,1)} fusion(bf16[768,2048]{1,0:T(8,128)(2,1)} %bitcast.24, s32[1024]{0:T(1024)S(1)} %pad_clamp_fusion), kind=kCustom, calls=%fused_computation.1 | custom fusion | bytes 4196352 | tf_op jit(solution)/shard_map/gather | solution.py:177
  312.3 4.7 %reshape.335 = f32[128,4,2048]{2,1,0:T(4,128)} reshape(bf16[512,2048]{1,0:T(8,128)(2,1)} %gather_fusion) | data formatting | bytes 6291456 | tf_op jit(solution)/shard_map/convert_element_type | solution.py:178
  317.0 5.4 %multiply_reduce_fusion = f32[128,2048]{1,0:T(8,128)S(1)} fusion(f32[128,4,2048]{2,1,0:T(4,128)} %reshape.335, f32[128,4]{1,0:T(8,128)S(1)} %copy.35), kind=kLoop, calls=%fused_computation.8 | loop fusion | flops 1835008 | bytes 5244928 | tf_op jit(solution)/shard_map/reduce_sum | solution.py:178
  322.4 0.0 reduce-scatter.2.cloned.1.call-done
  322.4 2.1 add_convert_fusion
  (27 shorter events, 0.4 us)
Async XLA Ops:
  7.2 157.3 %copy-start = (bf16[1,512,2048]{2,1,0:T(8,128)(2,1)S(1)}, bf16[1,512,2048]{2,1,0:T(8,128)(2,1)}, u32[]{:S(2)}) copy-start(bf16[1,512,2048]{2,1,0:T(8,128)(2,1)} %param.28) | copy-start | bytes 6291460
  7.2 3.5 %copy-start.5 = (s32[128,4]{0,1:T(4,128)S(1)}, s32[128,4]{0,1:T(4,128)}, u32[]{:S(2)}) copy-start(s32[128,4]{0,1:T(4,128)} %param.25) | copy-start | bytes 6148
  7.2 87.1 %all-gather.5.cloned.1.call-start = ((), (), s32[]{:S(2)}) async-start(), calls=%async_computation.4 | async-start | bytes 2621440 | tf_op jit(solution)/shard_map/all_gather | solution.py:115
  24.9 7.5 %copy-start.2 = (bf16[128,2048]{1,0:T(8,128)(2,1)S(1)}, bf16[128,2048]{1,0:T(8,128)(2,1)}, u32[]{:S(2)}) copy-start(bf16[128,2048]{1,0:T(8,128)(2,1)} %param.16) | copy-start | bytes 1572868
  24.9 7.7 %copy-start.6 = (f32[2048]{0:T(1024)S(1)}, f32[2048]{0:T(1024)}, u32[]{:S(2)}) copy-start(f32[2048]{0:T(1024)} %param.17) | copy-start | bytes 24580
  24.9 134.0 %all-to-all-start = ((bf16[16,48,2048]{2,1,0:T(8,128)(2,1)}), bf16[16,48,2048]{2,1,0:T(8,128)(2,1)}, u32[]{:S(2)}, u32[]{:S(2)}) async-start(bf16[16,48,2048]{2,1,0:T(8,128)(2,1)} %bitcast.76), calls=%async_computation | async-start | bytes 6291456 | tf_op jit(solution)/shard_map/all_to_all | solution.py:161
  32.4 61.9 %copy-start.3 = (bf16[2048,128]{1,0:T(8,128)(2,1)S(1)}, bf16[2048,128]{1,0:T(8,128)(2,1)}, u32[]{:S(2)}) copy-start(bf16[2048,128]{1,0:T(8,128)(2,1)} %param.29) | copy-start | bytes 1572868
  32.4 148.1 %all-gather.3.cloned.1.call-start = ((), (), s32[]{:S(2)}) async-start(), calls=%async_computation.3 | async-start | bytes 2621440 | tf_op jit(solution)/shard_map/all_gather | solution.py:114
  33.7 288.7 %reduce-scatter.2.cloned.1.call-start = ((), (), s32[]{:S(2)}) async-start(), calls=%async_computation.5 | async-start | bytes 5242880 | tf_op jit(solution)/shard_map/reduce_scatter | solution.py:123
  173.0 5.9 %copy-start.7 = (f32[4]{0:T(128)S(1)}, f32[4]{0:T(128)}, u32[]{:S(2)}) copy-start(f32[4]{0:T(128)} %param.21) | copy-start | bytes 52
  173.0 6.0 %copy-start.1 = (bf16[128,2048]{1,0:T(8,128)(2,1)S(1)}, bf16[128,2048]{1,0:T(8,128)(2,1)}, u32[]{:S(2)}) copy-start(bf16[128,2048]{1,0:T(8,128)(2,1)} %fusion.32) | copy-start | bytes 1572868
  173.0 6.0 %copy-start.4 = (bf16[2048,16]{0,1:T(8,128)(2,1)S(1)}, bf16[2048,16]{0,1:T(8,128)(2,1)}, u32[]{:S(2)}) copy-start(bf16[2048,16]{0,1:T(8,128)(2,1)} %param.24) | copy-start | bytes 196612
  173.0 131.8 %all-to-all-start.1 = ((bf16[16,48,2048]{2,1,0:T(8,128)(2,1)}), bf16[16,48,2048]{2,1,0:T(8,128)(2,1)}, u32[]{:S(2)}, u32[]{:S(2)}) async-start(bf16[16,48,2048]{2,1,0:T(8,128)(2,1)} %bitcast.77), calls=%async_computation.1 | async-start | bytes 6291456 | tf_op jit(solution)/shard_map/all_to_all | solution.py:168
  184.3 7.3 %collective-permute-start = (bf16[128,256]{0,1:T(8,128)(2,1)S(1)}, bf16[128,256]{0,1:T(8,128)(2,1)S(1)}, u32[]{:S(2)}, u32[]{:S(2)}) collective-permute-start(bf16[128,256]{0,1:T(8,128)(2,1)S(1)} %get-tuple-element.43), channel_id=1, source_target_pairs={{0,4},{4,8},{8,12},{1,5},{5,9},{9,13},{2,6},{6,10},{10,14},{3,7},{... | collective-permute-start | bytes 196616 | tf_op jit(solution)/shard_map/ppermute | solution.py:20
  187.9 6.1 %collective-permute-start.1 = (bf16[128,256]{0,1:T(8,128)(2,1)S(1)}, bf16[128,256]{0,1:T(8,128)(2,1)S(1)}, u32[]{:S(2)}, u32[]{:S(2)}) collective-permute-start(bf16[128,256]{0,1:T(8,128)(2,1)S(1)} %get-tuple-element.44), channel_id=1, source_target_pairs={{4,0},{8,4},{12,8},{5,1},{9,5},{13,9},{6,2},{10,6},{14,10},{7,3},{... | collective-permute-start | bytes 196616 | tf_op jit(solution)/shard_map/ppermute | solution.py:23
Sparse Core Ops, SparseCore 0:
  10.8 83.4 all-gather.4
  96.4 63.3 all-gather.2
  162.1 125.0 reduce-scatter.1
where the time goes:
time: 333 us; the launch traced here: 331 us
  waiting for transfers between devices  226 us (68%)
  matrix products  29.4 us (9%)
  local copies, waits for them, and re-layouts  26.3 us (8%)
  starting transfers between devices  19.4 us (6%)
  other arithmetic  16.3 us (5%)
  between operations  14 us (4%)
    all_to_all x1, waiting for transfers between devices, body(): lax.all_to_all(jnp.dot(hidden_rows, expert_down[0], preferred_element_typ...  105 us
    all_gather x1, waiting for transfers between devices, body(): lax.all_gather(normed_second, 'tp', axis=0, tiled=True)  60.4 us
    all_to_all x1, waiting for transfers between devices, body(): lax.all_to_all(outgoing, ('ep', 'tp'), split_axis=0, concat_axis=0, tiled...  56.2 us
    scatter x1, local copies, waits for them, and re-layouts, body(): outgoing = jnp.zeros((experts * capacity, normed_second.shape[1]), jnp.bf...  12.1 us
    dot_general x1, matrix products, body(): jnp.dot(hidden_rows, expert_down[0], preferred_element_type=jnp.float32)  8.5 us
    gather x1, local copies, waits for them, and re-layouts, body(): returned.reshape(experts * capacity, -1)[target]  7.52 us
    all_to_all x1, starting transfers between devices, body(): lax.all_to_all(outgoing, ('ep', 'tp'), split_axis=0, concat_axis=0, tiled...  7.47 us
  transfers between devices with their start and end apart: 7, of which 5 were waited for; matrix products, arithmetic and copies ran while one was open for 20% of the time, Pallas kernels for 0%

commit v1 on v0

--- a/solution.py
+++ b/solution.py
@@ -1,6 +1,10 @@
+import functools
+
 import jax
 import jax.numpy as jnp
 from jax import lax
+from jax.experimental import pallas as pl
+from jax.experimental.pallas import tpu as pltpu
 from jax.sharding import PartitionSpec as P
 
 HEAD_DIM = 64
@@ -85,6 +89,398 @@
 
     blocks_out = lax.map(one_block, jnp.arange(span_rows // block_rows, dtype=jnp.int32))
     return blocks_out.reshape(span_rows, head_count * head_width)
+
+
+MESH = pl.DeviceIdType.MESH
+VMEM_LIMIT = 60 * 2**20
+CHUNK = 512
+
+
+def remote(src, dst, send_sem, recv_sem, device):
+    return pltpu.make_async_remote_copy(
+        src_ref=src,
+        dst_ref=dst,
+        send_sem=send_sem,
+        recv_sem=recv_sem,
+        device_id=device,
+        device_id_type=MESH,
+    )
+
+
+def entry_barrier(grp, ep, tp, ep_count, tp_count):
+    barrier = pltpu.get_barrier_semaphore()
+
+    @pl.when(tp > 0)
+    def _():
+        pl.semaphore_signal(barrier, inc=1, device_id=(grp, ep, tp - 1), device_id_type=MESH)
+
+    @pl.when(tp < tp_count - 1)
+    def _():
+        pl.semaphore_signal(barrier, inc=1, device_id=(grp, ep, tp + 1), device_id_type=MESH)
+
+    for d in range(1, ep_count):
+        pl.semaphore_signal(
+            barrier, inc=1, device_id=(grp, lax.rem(ep + d, ep_count), tp), device_id_type=MESH
+        )
+
+    inner = (tp > 0) & (tp < tp_count - 1)
+    pl.semaphore_wait(barrier, ep_count + jnp.where(inner, 1, 0))
+
+
+def dispatch_kernel(
+    ep_count, tp_count, second, first, meta, gath2, gath1, metag, disp, sbuf,
+    own_sem, s2, r2, sm, rm, s1, r1, sd, rd, ld,
+):
+    grp, ep, tp = lax.axis_index("grp"), lax.axis_index("ep"), lax.axis_index("tp")
+    rows, width = second.shape
+    slots = disp.shape[2]
+    entry_barrier(grp, ep, tp, ep_count, tp_count)
+    locals_ = [
+        pltpu.make_async_copy(second, gath2.at[tp], own_sem.at[0]),
+        pltpu.make_async_copy(meta, metag.at[tp], own_sem.at[1]),
+        pltpu.make_async_copy(first, gath1.at[tp], own_sem.at[2]),
+    ]
+
+    def toward(side):
+        return (grp, ep, tp + (1 if side == 0 else -1))
+
+    def exists(side):
+        return tp < tp_count - 1 if side == 0 else tp > 0
+
+    def send_second(side, block, own):
+        return [
+            remote(second if own else gath2.at[block], gath2.at[block], s2.at[side, block], r2.at[block], toward(side)),
+            remote(meta if own else metag.at[block], metag.at[block], sm.at[side, block], rm.at[block], toward(side)),
+        ]
+
+    def send_first(side, block, own):
+        return remote(first if own else gath1.at[block], gath1.at[block], s1.at[side, block], r1.at[block], toward(side))
+
+    def start_own_first(side, step):
+        last = tp if side == 0 else tp_count - 1 - tp
+
+        @pl.when(exists(side) & (step == last))
+        def _():
+            send_first(side, tp, True).start()
+
+    def dispatch_copy(block, d):
+        return remote(
+            sbuf.at[block, pl.ds(d * slots, slots)], disp.at[ep, block], sd.at[block, d], rd.at[block, d],
+            (grp, lax.rem(ep + d, ep_count), tp),
+        )
+
+    def local_dispatch(block):
+        return pltpu.make_async_copy(sbuf.at[block, pl.ds(0, slots)], disp.at[ep, block], ld.at[block])
+
+    def process(block):
+        slot_ids = lax.broadcasted_iota(jnp.int32, (slots, rows), 0).astype(jnp.float32)
+        picks = []
+        for d in range(ep_count):
+            expert = lax.rem(ep + d, ep_count) * tp_count + tp
+            places = metag[block, pl.ds(expert, 1), :]
+            picks.append(jnp.where(slot_ids == places, 1.0, 0.0))
+        pick = jnp.concatenate(picks, axis=0).astype(jnp.bfloat16)
+
+        def columns(c, carry):
+            span = pl.ds(pl.multiple_of(c * CHUNK, CHUNK), CHUNK)
+            sbuf[block, :, span] = jnp.dot(
+                pick, gath2[block, :, span], preferred_element_type=jnp.float32
+            ).astype(jnp.bfloat16)
+            return carry
+
+        lax.fori_loop(0, width // CHUNK, columns, 0)
+        for d in range(1, ep_count):
+            dispatch_copy(block, d).start()
+        local_dispatch(block).start()
+
+    for side in range(2):
+
+        @pl.when(exists(side))
+        def _():
+            for copy in send_second(side, tp, True):
+                copy.start()
+
+        start_own_first(side, 0)
+    for copy in locals_:
+        copy.start()
+    locals_[0].wait()
+    locals_[1].wait()
+    process(tp)
+
+    def hop(k, carry):
+        for side in range(2):
+            block = tp - k if side == 0 else tp + k
+            inside = block >= 0 if side == 0 else block < tp_count
+
+            @pl.when(inside)
+            def _():
+                for copy in send_second(side, block, False):
+                    copy.wait_recv()
+
+                @pl.when(exists(side))
+                def _():
+                    for copy in send_second(side, block, False):
+                        copy.start()
+
+            start_own_first(side, k)
+
+            @pl.when(inside)
+            def _():
+                process(block)
+
+        return carry
+
+    lax.fori_loop(1, tp_count, hop, 0)
+    locals_[2].wait()
+
+    def hop_first(k, carry):
+        for side in range(2):
+            block = tp - k if side == 0 else tp + k
+            inside = block >= 0 if side == 0 else block < tp_count
+
+            @pl.when(inside)
+            def _():
+                send_first(side, block, False).wait_recv()
+
+                @pl.when(exists(side))
+                def _():
+                    send_first(side, block, False).start()
+
+        return carry
+
+    lax.fori_loop(1, tp_count, hop_first, 0)
+
+    def finish(block, carry):
+        for d in range(1, ep_count):
+            dispatch_copy(block, d).wait()
+        local_dispatch(block).wait()
+        for side in range(2):
+            passed = block <= tp if side == 0 else block >= tp
+
+            @pl.when(exists(side) & passed)
+            def _():
+                for copy in send_second(side, block, False):
+                    copy.wait_send()
+                send_first(side, block, False).wait_send()
+
+        return carry
+
+    lax.fori_loop(0, tp_count, finish, 0)
+
+
+def dispatch(second, first, meta, ep_count, tp_count, slots):
+    rows, width = second.shape
+    vmem = pl.BlockSpec(memory_space=pltpu.VMEM)
+    dma = pltpu.SemaphoreType.DMA
+    return pl.pallas_call(
+        functools.partial(dispatch_kernel, ep_count, tp_count),
+        out_shape=(
+            jax.ShapeDtypeStruct((tp_count, rows, width), jnp.bfloat16),
+            jax.ShapeDtypeStruct((tp_count, rows, width), jnp.bfloat16),
+            jax.ShapeDtypeStruct((tp_count,) + meta.shape, jnp.float32),
+            jax.ShapeDtypeStruct((ep_count, tp_count, slots, width), jnp.bfloat16),
+        ),
+        in_specs=[vmem] * 3,
+        out_specs=(vmem,) * 4,
+        scratch_shapes=[
+            pltpu.VMEM((tp_count, ep_count * slots, width), jnp.bfloat16),
+            dma((3,)),
+            dma((2, tp_count)),
+            dma((tp_count,)),
+            dma((2, tp_count)),
+            dma((tp_count,)),
+            dma((2, tp_count)),
+            dma((tp_count,)),
+            dma((tp_count, ep_count)),
+            dma((tp_count, ep_count)),
+            dma((tp_count,)),
+        ],
+        compiler_params=pltpu.CompilerParams(
+            collective_id=0, has_side_effects=True, vmem_limit_bytes=VMEM_LIMIT
+        ),
+        name="dispatch",
+    )(second, first, meta)
+
+
+def combine_kernel(
+    ep_count, tp_count, results, hidden, down, metag, out, back, rin, lin, psend,
+    sb, rb, lb, sp, rr, rl,
+):
+    grp, ep, tp = lax.axis_index("grp"), lax.axis_index("ep"), lax.axis_index("tp")
+    rows, width = out.shape
+    slots = results.shape[2]
+    experts = metag.shape[1] // 2
+    entry_barrier(grp, ep, tp, ep_count, tp_count)
+
+    def return_copy(block, d):
+        target = lax.rem(ep + d, ep_count)
+        return remote(
+            results.at[target, block], back.at[block, pl.ds(d * slots, slots)], sb.at[block, d], rb.at[block, d],
+            (grp, target, tp),
+        )
+
+    def local_return(block):
+        return pltpu.make_async_copy(results.at[ep, block], back.at[block, pl.ds(0, slots)], lb.at[block])
+
+    def start_return(block):
+        for d in range(1, ep_count):
+            return_copy(block, d).start()
+        local_return(block).start()
+
+    def wait_return(block):
+        for d in range(1, ep_count):
+            return_copy(block, d).wait_recv()
+        local_return(block).wait()
+
+    def pass_on(side, block):
+        return remote(
+            psend.at[block],
+            (rin if side == 0 else lin).at[block],
+            sp.at[block],
+            (rr if side == 0 else rl).at[block],
+            (grp, ep, tp + (1 if side == 0 else -1)),
+        )
+
+    def begin(k, carry):
+        @pl.when(tp_count - 1 - k > tp)
+        def _():
+            start_return(tp_count - 1 - k)
+
+        @pl.when(k < tp)
+        def _():
+            start_return(k)
+
+        return carry
+
+    lax.fori_loop(0, tp_count - 1, begin, 0)
+    start_return(tp)
+
+    @pl.when(tp == 0)
+    def _():
+        rin[...] = jnp.zeros_like(rin)
+
+    @pl.when(tp == tp_count - 1)
+    def _():
+        lin[...] = jnp.zeros_like(lin)
+
+    def mixing(block):
+        slot_ids = lax.broadcasted_iota(jnp.int32, (slots, rows), 0).astype(jnp.float32)
+        parts = []
+        for d in range(ep_count):
+            expert = lax.rem(ep + ep_count - d, ep_count) * tp_count + tp
+            places = metag[block, pl.ds(expert, 1), :]
+            scales = metag[block, pl.ds(experts + expert, 1), :]
+            parts.append(jnp.where(slot_ids == places, scales, 0.0))
+        weights = jnp.concatenate(parts, axis=0)
+        high = weights.astype(jnp.bfloat16)
+        low = (weights - high.astype(jnp.float32)).astype(jnp.bfloat16)
+        return high, low
+
+    def partial(block, high, low, span):
+        picked = back[block, :, span]
+        turned = (((0,), (0,)), ((), ()))
+        return (
+            lax.dot_general(high, picked, turned, preferred_element_type=jnp.float32)
+            + lax.dot_general(low, picked, turned, preferred_element_type=jnp.float32)
+            + jnp.dot(hidden[block], down[:, span], preferred_element_type=jnp.float32)
+        )
+
+    def reduce_step(k, carry):
+        for side in range(2):
+            block = tp_count - 1 - k if side == 0 else k
+            active = block > tp if side == 0 else block < tp
+            arrived = rin if side == 0 else lin
+
+            @pl.when(active)
+            def _():
+                wait_return(block)
+
+                @pl.when(tp > 0 if side == 0 else tp < tp_count - 1)
+                def _():
+                    pass_on(side, block).wait_recv()
+
+                high, low = mixing(block)
+
+                def columns(c, inner):
+                    span = pl.ds(pl.multiple_of(c * CHUNK, CHUNK), CHUNK)
+                    psend[block, :, span] = (
+                        partial(block, high, low, span) + arrived[block, :, span].astype(jnp.float32)
+                    ).astype(jnp.bfloat16)
+                    return inner
+
+                lax.fori_loop(0, width // CHUNK, columns, 0)
+                pass_on(side, block).start()
+
+        return carry
+
+    lax.fori_loop(0, tp_count - 1, reduce_step, 0)
+    wait_return(tp)
+
+    @pl.when(tp > 0)
+    def _():
+        pass_on(0, tp).wait_recv()
+
+    @pl.when(tp < tp_count - 1)
+    def _():
+        pass_on(1, tp).wait_recv()
+
+    high, low = mixing(tp)
+
+    def columns(c, carry):
+        span = pl.ds(pl.multiple_of(c * CHUNK, CHUNK), CHUNK)
+        out[:, span] = (
+            partial(tp, high, low, span)
+            + rin[tp, :, span].astype(jnp.float32)
+            + lin[tp, :, span].astype(jnp.float32)
+        ).astype(jnp.bfloat16)
+        return carry
+
+    lax.fori_loop(0, width // CHUNK, columns, 0)
+
+    def finish(block, carry):
+        for d in range(1, ep_count):
+            return_copy(block, d).wait_send()
+
+        @pl.when(block > tp)
+        def _():
+            pass_on(0, block).wait_send()
+
+        @pl.when(block < tp)
+        def _():
+            pass_on(1, block).wait_send()
+
+        return carry
+
+    lax.fori_loop(0, tp_count, finish, 0)
+
+
+def combine(results, hidden, down, metag):
+    ep_count, tp_count, slots, width = results.shape
+    rows = hidden.shape[1]
+    vmem = pl.BlockSpec(memory_space=pltpu.VMEM)
+    dma = pltpu.SemaphoreType.DMA
+    return pl.pallas_call(
+        functools.partial(combine_kernel, ep_count, tp_count),
+        out_shape=jax.ShapeDtypeStruct((rows, width), jnp.bfloat16),
+        in_specs=[vmem] * 4,
+        out_specs=vmem,
+        scratch_shapes=[
+            pltpu.VMEM((tp_count, ep_count * slots, width), jnp.bfloat16),
+            pltpu.VMEM((tp_count, rows, width), jnp.bfloat16),
+            pltpu.VMEM((tp_count, rows, width), jnp.bfloat16),
+            pltpu.VMEM((tp_count, rows, width), jnp.bfloat16),
+            dma((tp_count, ep_count)),
+            dma((tp_count, ep_count)),
+            dma((tp_count,)),
+            dma((tp_count,)),
+            dma((tp_count,)),
+            dma((tp_count,)),
+        ],
+        compiler_params=pltpu.CompilerParams(
+            collective_id=1, has_side_effects=True, vmem_limit_bytes=VMEM_LIMIT
+        ),
+        name="combine",
+    )(results, hidden, down, metag)
 
 
 def body(
@@ -105,30 +501,53 @@
     shared_up,
     shared_down,
 ):
+    tokens = mixer_in.shape[0]
+    ep_count, tp_count = lax.axis_size("ep"), lax.axis_size("tp")
+    top_count = routes.shape[1]
+    experts = router.shape[1]
+    capacity = 3 * top_count * tokens // (2 * experts)
+    slots = -(-capacity // 16) * 16
+    normed_second = rms_rows(moe_in, moe_gain)
     normed_first = rms_rows(mixer_in, mixer_gain)
-    normed_second = rms_rows(moe_in, moe_gain)
-    query_cols = w_query.shape[1]
-    key_cols = w_key.shape[1]
-    joined = jnp.concatenate([w_query, w_key, w_value], axis=1)
-    gathered_first, gathered_second = (
-        lax.all_gather(normed_first, "tp", axis=0, tiled=True),
-        lax.all_gather(normed_second, "tp", axis=0, tiled=True),
-    )
-    projected = jnp.dot(gathered_first, joined, preferred_element_type=jnp.float32)
-    row_block = gathered_second
+    affinity = jax.nn.sigmoid(jnp.dot(normed_second, router, preferred_element_type=jnp.float32))
+    hits = jnp.any(
+        routes[:, :, None] == jnp.arange(experts, dtype=jnp.int32)[None, None, :], axis=1
+    )
+    chosen = jnp.where(hits, affinity, 0.0)
+    route_weight = ROUTED_SCALE * chosen / jnp.sum(chosen, axis=-1, keepdims=True)
+    earlier = jnp.tril(jnp.ones((tokens, tokens), jnp.bfloat16), -1)
+    before = jnp.dot(earlier, hits.astype(jnp.bfloat16), preferred_element_type=jnp.float32)
+    places = jnp.where(hits, before, -1.0)
+    meta = jnp.concatenate([places, route_weight], axis=1).T
+    gathered_second, gathered_first, metag, arrived = dispatch(
+        normed_second, normed_first, meta, ep_count, tp_count, slots
+    )
+    width = normed_second.shape[1]
+    flat_rows = arrived.reshape(-1, width)
+    hidden_rows = (
+        jax.nn.silu(jnp.dot(flat_rows, expert_gate[0], preferred_element_type=jnp.float32))
+        * jnp.dot(flat_rows, expert_up[0], preferred_element_type=jnp.float32)
+    ).astype(jnp.bfloat16)
+    results = (
+        jnp.dot(hidden_rows, expert_down[0], preferred_element_type=jnp.float32)
+        .astype(jnp.bfloat16)
+        .reshape(arrived.shape)
+    )
+    row_block = gathered_second.reshape(-1, width)
     hidden = (
         jax.nn.silu(jnp.dot(row_block, shared_gate, preferred_element_type=jnp.float32))
         * jnp.dot(row_block, shared_up, preferred_element_type=jnp.float32)
     ).astype(jnp.bfloat16)
-    shared = lax.psum_scatter(
-        jnp.dot(hidden, shared_down, preferred_element_type=jnp.float32),
-        "tp",
-        scatter_dimension=0,
-        tiled=True,
+    moe_out = combine(results, hidden.reshape(tp_count, tokens, -1), shared_down, metag)
+    query_cols = w_query.shape[1]
+    key_cols = w_key.shape[1]
+    joined = jnp.concatenate([w_query, w_key, w_value], axis=1)
+    projected = jnp.dot(
+        gathered_first.reshape(-1, width), joined, preferred_element_type=jnp.float32
     )
     span_rows = projected.shape[0]
     offset = lax.axis_index("ep") * span_rows
-    seq_length = span_rows * lax.axis_size("ep")
+    seq_length = span_rows * ep_count
     positions = offset + jnp.arange(span_rows, dtype=jnp.int32)
     query_rows = rotate(
         projected[:, :query_cols].reshape(span_rows, -1, HEAD_DIM), positions
@@ -140,43 +559,6 @@
     stacked = jnp.concatenate([key_rows.reshape(span_rows, key_cols), value_rows], axis=1)
     padded = extended(stacked, (("ep", 0),), WINDOW)
     mixed = attend(query_rows, padded, sink_logit, offset, seq_length)
-    tokens = normed_second.shape[0]
-    top_count = routes.shape[1]
-    experts = router.shape[1]
-    capacity = 3 * top_count * tokens // (2 * experts)
-    affinity = jax.nn.sigmoid(jnp.dot(normed_second, router, preferred_element_type=jnp.float32))
-    hit_table = routes[:, :, None] == jnp.arange(experts, dtype=jnp.int32)[None, None, :]
-    chosen = jnp.sum(jnp.where(hit_table, affinity[:, None, :], 0.0), axis=-1)
-    route_weight = ROUTED_SCALE * chosen / jnp.sum(chosen, axis=-1, keepdims=True)
-    flat_hits = hit_table.reshape(tokens * top_count, experts).astype(jnp.int32)
-    slot_index = jnp.sum((jnp.cumsum(flat_hits, axis=0) - 1) * flat_hits, axis=-1)
-    target = routes.reshape(-1) * capacity + slot_index
-    source = jnp.arange(tokens * top_count, dtype=jnp.int32) // top_count
-    outgoing = (
-        jnp.zeros((experts * capacity, normed_second.shape[1]), jnp.bfloat16)
-        .at[target]
-        .set(normed_second[source])
-    )
-    outgoing = outgoing.reshape(experts, capacity, -1)
-    row_block = lax.all_to_all(outgoing, ("ep", "tp"), split_axis=0, concat_axis=0, tiled=True)
-    row_shape = row_block.shape
-    flat_rows = row_block.reshape(-1, row_shape[-1])
-    hidden_rows = (
-        jax.nn.silu(jnp.dot(flat_rows, expert_gate[0], preferred_element_type=jnp.float32))
-        * jnp.dot(flat_rows, expert_up[0], preferred_element_type=jnp.float32)
-    ).astype(jnp.bfloat16)
-    returned = lax.all_to_all(
-        jnp.dot(hidden_rows, expert_down[0], preferred_element_type=jnp.float32)
-        .astype(jnp.bfloat16)
-        .reshape(row_shape),
-        ("ep", "tp"),
-        split_axis=0,
-        concat_axis=0,
-        tiled=True,
-    )
-    picked = returned.reshape(experts * capacity, -1)[target].reshape(tokens, top_count, -1)
-    routed = jnp.sum(picked.astype(jnp.float32) * route_weight[:, :, None], axis=1)
-    moe_out = (routed + shared).astype(jnp.bfloat16)
     return (mixed, moe_out)
 
 

time: 333 us -> 186 us (0.56)
  waiting for transfers between devices: 226 us -> 0.01 us
  Pallas kernels: 0 us -> 140 us
  local copies, waits for them, and re-layouts: 26.3 us -> 3.02 us
  between operations: 14 us -> 0.94 us
  starting transfers between devices: 19.4 us -> 8.34 us
  matrix products: 29.4 us -> 22.1 us
  other arithmetic: 16.3 us -> 11.5 us
    all_to_all x2 -> x0, waiting for transfers between devices: 161 us -> none  [the longest x1 105 us: body(): lax.all_to_all(jnp.dot(hidden_rows, expert_down[0], preferred_element_typ...]
    pallas_call x0 -> x2, Pallas kernels: none -> 140 us  [the longest x1 77.3 us: dispatch(): pl.pallas_call(functools.partial(dispatch_kernel, ep_count, tp_count), ou...]
    all_gather x2 -> x0, waiting for transfers between devices: 60.4 us -> none  [the longest x1 60.4 us: body(): lax.all_gather(normed_second, 'tp', axis=0, tiled=True)]
    all_to_all x2 -> x0, starting transfers between devices: 13.3 us -> none  [the longest x1 7.47 us: body(): lax.all_to_all(outgoing, ('ep', 'tp'), split_axis=0, concat_axis=0, tiled...]
    scatter x1 -> x0, local copies, waits for them, and re-layouts: 12.1 us -> none  [body(): outgoing = jnp.zeros((experts * capacity, normed_second.shape[1]), jnp.bf...]
    gather x1 -> x0, local copies, waits for them, and re-layouts: 7.52 us -> none  [body(): returned.reshape(experts * capacity, -1)[target]]
    reduce_sum x3 -> x0, other arithmetic: 5.5 us -> none  [the longest x1 5.35 us: body(): jnp.sum(picked.astype(jnp.float32) * route_weight[:, :, None], axis=1)]
    convert_element_type x1 -> x0, local copies, waits for them, and re-layouts: 4.73 us -> none  [body(): picked.astype(jnp.float32) * route_weight[:, :, None]]
  transfers between devices with their start and end apart: 7 -> 2, of which waited for: 5 -> 0; matrix products, arithmetic and copies ran while one was open for 20% -> 9% of each run, Pallas kernels for 0% -> 34%
where the time goes in v1:
time: 186 us
  Pallas kernels  140 us (75%)
  matrix products  22.1 us (12%)
  other arithmetic  11.5 us (6%)
  starting transfers between devices  8.34 us (4%)
  local copies, waits for them, and re-layouts  3.02 us (2%)
    pallas_call x1, Pallas kernels, dispatch(): pl.pallas_call(functools.partial(dispatch_kernel, ep_count, tp_count), ou...  77.3 us
    pallas_call x1, Pallas kernels, combine(): pl.pallas_call(functools.partial(combine_kernel, ep_count, tp_count), out...  62.7 us
    dot_general x1, matrix products, body(): jnp.dot(hidden_rows, expert_down[0], preferred_element_type=jnp.float32)  8.16 us
    ppermute x1, starting transfers between devices, extended(): lax.ppermute(lax.slice_in_dim(block, block.shape[dim] - width, None, axis...  6.42 us
  transfers between devices with their start and end apart: 2, of which 0 were waited for; matrix products, arithmetic and copies ran while one was open for 9% of the time, Pallas kernels for 34%

profile of v1, /device:TPU:1, one launch (start us, length us, event | category | flops | bytes accessed | tf_op | source)
XLA Modules:
  0.0 185.9 jit_solution(14513113465666607641)
XLA Ops:
  0.6 0.0 copy-start
  0.6 0.0 copy-start.7
  0.7 1.4 fusion.27
  2.1 1.2 fusion.24
  3.3 0.7 fusion.39
  4.0 0.2 convolution_select_fusion
  4.2 2.2 %fusion.26 = (bf16[128,2048]{1,0:T(8,128)(2,1)S(1)}, bf16[128,2048]{1,0:T(8,128)(2,1)}) fusion(bf16[128,2048]{1,0:T(8,128)(2,1)} %param.22, f32[2048]{0:T(1024)} %param.23, f32[128]{0:T(128)S(1)} %add_rsqrt_fusion.1, f32[2048]{0:T(1024)} %param.17, f32[128]{0:T(128)S(1)} %add_rsqrt_fusion, bf16[128,2048]{1,0:T(8,128)(2,1)} %param.16), kind=kLoop, calls=%fused_computation.37 | loop fusion | flops 2097152 | bytes 2114560 | tf_op jit(solution)/shard_map/convert_element_type | solution.py:35
  6.4 0.0 copy-start.1
  6.4 0.0 copy-done.7
  6.4 0.3 fusion.53
  6.7 0.6 maximum_bitcast_fusion.meta
  7.4 0.0 copy-done.1
  7.4 77.3 %dispatch.1 = (bf16[4,128,2048]{2,1,0:T(8,128)(2,1)}, bf16[4,128,2048]{2,1,0:T(8,128)(2,1)}, f32[4,32,128]{2,1,0:T(8,128)}, bf16[4,4,48,2048]{3,2,1,0:T(8,128)(2,1)}) custom-call(bf16[128,2048]{1,0:T(8,128)(2,1)} %copy-done.1, bf16[128,2048]{1,0:T(8,128)(2,1)} %get-tuple-element.56.first, f32[32,128]{1,0:T(8,128)} %maximum_bitcast_fusion.meta), custom_call_target="tpu_custom_call" | custom-call | tf_op jit(solution)/shard_map/dispatch/pallas_call | solution.py:275
  84.6 3.5 %fusion.3 = f32[512,512]{0,1:T(8,128)S(1)} fusion(bf16[512,2048]{1,0:T(8,128)(2,1)} %bitcast.76, bf16[2048,128]{1,0:T(8,128)(2,1)} %param.20, bf16[2048,128]{1,0:T(8,128)(2,1)} %param.19, bf16[2048,256]{1,0:T(8,128)(2,1)} %param.18), kind=kOutput, calls=%fused_computation.7 | convolution fusion | flops 1080033280 | bytes 5242880 | tf_op jit(solution)/shard_map/dot_general | solution.py:545
  88.2 0.3 multiply_cosine_fusion
  88.5 0.0 copy-start.4
  88.5 0.0 copy-start.5
  88.6 0.5 copy-done.4
  89.1 0.0 copy-done.5
  89.2 0.6 pad_maximum_fusion.3
  89.8 6.4 %collective-permute-start = (bf16[128,256]{0,1:T(8,128)(2,1)}, bf16[128,256]{0,1:T(8,128)(2,1)}, u32[]{:S(2)}, u32[]{:S(2)}) collective-permute-start(bf16[128,256]{0,1:T(8,128)(2,1)} %get-tuple-element.47), channel_id=1, source_target_pairs={{0,4},{4,8},{8,12},{1,5},{5,9},{9,13},{2,6},{6,10},{10,14},{3,7},{... | collective-permute-start | bytes 196616 | tf_op jit(solution)/shard_map/ppermute | solution.py:24
  96.2 1.9 %collective-permute-start.1 = (bf16[128,256]{0,1:T(8,128)(2,1)}, bf16[128,256]{0,1:T(8,128)(2,1)}, u32[]{:S(2)}, u32[]{:S(2)}) collective-permute-start(bf16[128,256]{0,1:T(8,128)(2,1)} %get-tuple-element.48), channel_id=1, source_target_pairs={{4,0},{8,4},{12,8},{5,1},{9,5},{13,9},{6,2},{10,6},{14,10},{7,3},{... | collective-permute-start | bytes 196616 | tf_op jit(solution)/shard_map/ppermute | solution.py:27
  98.2 0.0 copy-start.6
  98.2 0.0 copy-start.10
  98.3 0.0 copy-start.3
  98.3 1.1 subtract_convert_fusion
  99.4 0.0 copy-done.6
  99.4 0.0 copy-start.9
  99.4 2.4 %fusion.54 = f32[512,128]{1,0:T(8,128)S(1)} fusion(bf16[512,2048]{1,0:T(8,128)(2,1)} %bitcast.63, bf16[2048,128]{1,0:T(8,128)(2,1)S(1)} %copy-done.6), kind=kOutput, calls=%fused_computation.85 | convolution fusion | flops 268435456 | bytes 2883584 | tf_op jit(solution)/shard_map/dot_general | solution.py:538
  101.9 0.0 copy-done.10
  101.9 0.0 copy-done.3
  101.9 0.0 copy-start.8
  101.9 1.4 fusion.19
  103.3 0.0 copy-done.9
  103.3 0.6 copy-done.8
  103.8 2.9 %fusion.12 = f32[768,512]{1,0:T(8,128)} fusion(bf16[768,2048]{1,0:T(8,128)(2,1)S(1)} %bitcast.75, bf16[1,2048,512]{2,1,0:T(8,128)(2,1)S(1)} %copy-done.9), kind=kOutput, calls=%fused_computation.16 | convolution fusion | flops 1610612736 | bytes 6815744 | tf_op jit(solution)/shard_map/dot_general | solution.py:528
  106.7 0.0 copy-done
  106.7 0.0 copy-start.11
  106.7 8.2 %convolution_convert_fusion = bf16[768,2048]{1,0:T(8,128)(2,1)} fusion(bf16[1,512,2048]{2,1,0:T(8,128)(2,1)S(1)} %copy-done, f32[768,512]{1,0:T(8,128)} %fusion.12, bf16[768,2048]{1,0:T(8,128)(2,1)} %bitcast.74, bf16[1,2048,512]{2,1,0:T(8,128)(2,1)} %param.27), kind=kOutput, calls=%fused_computation.5 | convolution fusion | flops 3225157632 | bytes 12058624 | tf_op jit(solution)/shard_map/dot_general | solution.py:532
  114.9 0.7 fusion.15
  115.7 0.0 copy-done.11
  115.7 0.1 max.22
  115.7 62.7 %combine.1 = bf16[128,2048]{1,0:T(8,128)(2,1)} custom-call(bf16[4,4,48,2048]{3,2,1,0:T(8,128)(2,1)} %bitcast.61, bf16[4,128,128]{2,1,0:T(8,128)(2,1)} %bitcast.73, bf16[128,2048]{1,0:T(8,128)(2,1)} %down.1, f32[4,32,128]{2,1,0:T(8,128)} %get-tuple-element.36.metag), custom_call_target="tpu_custom_call" | custom-call | tf_op jit(solution)/shard_map/combine/pallas_call | solution.py:462
  178.5 0.0 collective-permute-done
  178.5 0.0 collective-permute-done.1
  178.5 0.9 pad_maximum_fusion
  179.5 1.3 fusion.1
  180.7 0.1 broadcast_maximum_fusion
  180.8 1.4 fusion
  182.2 0.1 exponential_add_fusion
  182.3 0.0 copy-start.2
  182.3 2.0 %fusion.18 = bf16[2,64,2,512]{3,1,2,0:T(8,128)(2,1)S(1)} fusion(bf16[768,2,64,1]{0,2,3,1:T(8,128)(2,1)S(1)} %bitcast.69, f32[2,768,512,2]{2,1,3,0:T(8,128)S(1)} %get-tuple-element.54, f32[2,2,512]{2,1,0:T(2,128)S(1)} %exponential_add_fusion, f32[2,2,512]{2,1,0:T(2,128)S(1)} %broadcast_maximum_fusion, pred[512,768]{0,1:T(8,128)(4,1)S(1)} %fusion.15), kind=kOutput, calls=%fused_computation.26 | convolution fusion | flops 209321984 | bytes 7159808 | tf_op jit(solution)/shard_map/while/body/eval_jaxpr/kgqc,ckd->qkgd/dot_general | solution.py:85
  184.3 0.8 copy.22
  185.1 0.0 copy-done.2
  185.1 0.8 copy.27
  (14 shorter events, 0.2 us)
Async XLA Ops:
  0.6 106.1 %copy-start = (bf16[1,512,2048]{2,1,0:T(8,128)(2,1)S(1)}, bf16[1,512,2048]{2,1,0:T(8,128)(2,1)}, u32[]{:S(2)}) copy-start(bf16[1,512,2048]{2,1,0:T(8,128)(2,1)} %param.28) | copy-start | bytes 6291460
  0.6 5.8 %copy-start.7 = (bf16[2048,16]{0,1:T(8,128)(2,1)S(1)}, bf16[2048,16]{0,1:T(8,128)(2,1)}, u32[]{:S(2)}) copy-start(bf16[2048,16]{0,1:T(8,128)(2,1)} %param.24) | copy-start | bytes 196612
  6.4 0.9 copy-start.1
  88.5 0.6 copy-start.4
  88.5 0.6 copy-start.5
  89.8 88.7 %collective-permute-start = (bf16[128,256]{0,1:T(8,128)(2,1)}, bf16[128,256]{0,1:T(8,128)(2,1)}, u32[]{:S(2)}, u32[]{:S(2)}) collective-permute-start(bf16[128,256]{0,1:T(8,128)(2,1)} %get-tuple-element.47), channel_id=1, source_target_pairs={{0,4},{4,8},{8,12},{1,5},{5,9},{9,13},{2,6},{6,10},{10,14},{3,7},{... | collective-permute-start | bytes 196616 | tf_op jit(solution)/shard_map/ppermute | solution.py:24
  96.2 82.3 %collective-permute-start.1 = (bf16[128,256]{0,1:T(8,128)(2,1)}, bf16[128,256]{0,1:T(8,128)(2,1)}, u32[]{:S(2)}, u32[]{:S(2)}) collective-permute-start(bf16[128,256]{0,1:T(8,128)(2,1)} %get-tuple-element.48), channel_id=1, source_target_pairs={{4,0},{8,4},{12,8},{5,1},{9,5},{13,9},{6,2},{10,6},{14,10},{7,3},{... | collective-permute-start | bytes 196616 | tf_op jit(solution)/shard_map/ppermute | solution.py:27
  98.2 1.2 copy-start.6
  98.2 3.6 %copy-start.10 = (bf16[2048,128]{1,0:T(8,128)(2,1)S(1)}, bf16[2048,128]{1,0:T(8,128)(2,1)}, u32[]{:S(2)}) copy-start(bf16[2048,128]{1,0:T(8,128)(2,1)} %param.30) | copy-start | bytes 1572868
  98.3 3.6 %copy-start.3 = (bf16[4,128,2048]{2,1,0:T(8,128)(2,1)S(1)}, bf16[4,128,2048]{2,1,0:T(8,128)(2,1)}, u32[]{:S(2)}) copy-start(bf16[4,128,2048]{2,1,0:T(8,128)(2,1)} %get-tuple-element.26) | copy-start | bytes 6291460
  99.4 3.9 %copy-start.9 = (bf16[1,2048,512]{2,1,0:T(8,128)(2,1)S(1)}, bf16[1,2048,512]{2,1,0:T(8,128)(2,1)}, u32[]{:S(2)}) copy-start(bf16[1,2048,512]{2,1,0:T(8,128)(2,1)} %param.26) | copy-start | bytes 6291460
  101.9 1.9 %copy-start.8 = (bf16[4,4,48,2048]{3,2,1,0:T(8,128)(2,1)S(1)}, bf16[4,4,48,2048]{3,2,1,0:T(8,128)(2,1)}, u32[]{:S(2)}) copy-start(bf16[4,4,48,2048]{3,2,1,0:T(8,128)(2,1)} %get-tuple-element.25) | copy-start | bytes 9437188
  106.7 8.9 %copy-start.11 = (f32[4]{0:T(128)S(1)}, f32[4]{0:T(128)}, u32[]{:S(2)}) copy-start(f32[4]{0:T(128)} %param.21) | copy-start | bytes 52
  182.3 2.9 %copy-start.2 = (bf16[128,2048]{1,0:T(8,128)(2,1)S(1)}, bf16[128,2048]{1,0:T(8,128)(2,1)}, u32[]{:S(2)}) copy-start(bf16[128,2048]{1,0:T(8,128)(2,1)} %combine.1) | copy-start | bytes 1572868

commit v2 on v0

--- a/solution.py
+++ b/solution.py
@@ -1,6 +1,10 @@
+import functools
+
 import jax
 import jax.numpy as jnp
 from jax import lax
+from jax.experimental import pallas as pl
+from jax.experimental.pallas import tpu as pltpu
 from jax.sharding import PartitionSpec as P
 
 HEAD_DIM = 64
@@ -87,6 +91,384 @@
     return blocks_out.reshape(span_rows, head_count * head_width)
 
 
+MESH = pl.DeviceIdType.MESH
+VMEM_LIMIT = 63 * 2**20
+CHUNK = 512
+
+
+def remote(src, dst, send_sem, recv_sem, device):
+    return pltpu.make_async_remote_copy(
+        src_ref=src,
+        dst_ref=dst,
+        send_sem=send_sem,
+        recv_sem=recv_sem,
+        device_id=device,
+        device_id_type=MESH,
+    )
+
+
+def entry_barrier(grp, ep, tp, ep_count, tp_count):
+    barrier = pltpu.get_barrier_semaphore()
+
+    @pl.when(tp > 0)
+    def _():
+        pl.semaphore_signal(barrier, inc=1, device_id=(grp, ep, tp - 1), device_id_type=MESH)
+
+    @pl.when(tp < tp_count - 1)
+    def _():
+        pl.semaphore_signal(barrier, inc=1, device_id=(grp, ep, tp + 1), device_id_type=MESH)
+
+    for d in range(1, ep_count):
+        pl.semaphore_signal(
+            barrier, inc=1, device_id=(grp, lax.rem(ep + d, ep_count), tp), device_id_type=MESH
+        )
+
+    inner = (tp > 0) & (tp < tp_count - 1)
+    pl.semaphore_wait(barrier, ep_count + jnp.where(inner, 1, 0))
+
+
+def layer_kernel(
+    ep_count, tp_count, slots,
+    second, first, meta, gate_hbm, up_hbm, down_hbm, sgate, sup, sdown,
+    out, gath1,
+    gath2, metag, sbuf, disp, back, sides, psend, gate, up, down, hidden, hexp,
+    own_sem, w_sem, s2, r2, sm, rm, s1, r1, sd, rd, sb, rb, sp, rs,
+):
+    grp, ep, tp = lax.axis_index("grp"), lax.axis_index("ep"), lax.axis_index("tp")
+    rows, width = second.shape
+    experts = meta.shape[0] // 2
+    total = ep_count * slots
+    entry_barrier(grp, ep, tp, ep_count, tp_count)
+    own_copies = [
+        pltpu.make_async_copy(second, gath2.at[tp], own_sem.at[0]),
+        pltpu.make_async_copy(meta, metag.at[tp], own_sem.at[1]),
+        pltpu.make_async_copy(first, gath1.at[tp], own_sem.at[2]),
+    ]
+    weight_copies = [
+        pltpu.make_async_copy(gate_hbm.at[0], gate, w_sem.at[0]),
+        pltpu.make_async_copy(up_hbm.at[0], up, w_sem.at[1]),
+        pltpu.make_async_copy(down_hbm.at[0], down, w_sem.at[2]),
+    ]
+
+    def toward(side):
+        return (grp, ep, tp + (1 if side == 0 else -1))
+
+    def exists(side):
+        return tp < tp_count - 1 if side == 0 else tp > 0
+
+    def peer(d):
+        return (grp, lax.rem(ep + d, ep_count), tp)
+
+    def spans(body, size=CHUNK, extent=width):
+        def step(c, carry):
+            body(pl.ds(pl.multiple_of(c * size, size), size))
+            return carry
+
+        lax.fori_loop(0, extent // size, step, 0)
+
+    def send_second(side, block, own):
+        return [
+            remote(second if own else gath2.at[block], gath2.at[block], s2.at[side, block], r2.at[block], toward(side)),
+            remote(meta if own else metag.at[block], metag.at[block], sm.at[side, block], rm.at[block], toward(side)),
+        ]
+
+    def send_first(side, block, own):
+        return remote(first if own else gath1.at[block], gath1.at[block], s1.at[side, block], r1.at[block], toward(side))
+
+    def start_own_first(side, step):
+        last = tp if side == 0 else tp_count - 1 - tp
+
+        @pl.when(exists(side) & (step == last))
+        def _():
+            send_first(side, tp, True).start()
+
+    def dispatch_copy(block, d):
+        part = pl.ds(d * slots, slots)
+        return remote(sbuf.at[block, part], disp.at[block, part], sd.at[block, d], rd.at[block, d], peer(d))
+
+    def return_copy(block, d):
+        part = pl.ds(d * slots, slots)
+        return remote(sbuf.at[block, part], back.at[block, part], sb.at[block, d], rb.at[block, d], peer(ep_count - d))
+
+    def pass_on(side, block):
+        return remote(psend.at[block], sides.at[side, block], sp.at[block], rs.at[side, block], toward(side))
+
+    def places_of(block, d):
+        expert = lax.rem(ep + d, ep_count) * tp_count + tp
+        slot_ids = lax.broadcasted_iota(jnp.int32, (slots, rows), 0).astype(jnp.float32)
+        return slot_ids == metag[block, pl.ds(expert, 1), :], expert
+
+    def process(block):
+        picks = [jnp.where(places_of(block, d)[0], 1.0, 0.0) for d in range(ep_count)]
+        pick = jnp.concatenate(picks, axis=0).astype(jnp.bfloat16)
+
+        def columns(span):
+            picked = jnp.dot(pick, gath2[block, :, span], preferred_element_type=jnp.float32).astype(jnp.bfloat16)
+            disp[block, 0:slots, span] = picked[0:slots]
+            sbuf[block, slots:total, span] = picked[slots:total]
+
+        spans(columns)
+        for d in range(1, ep_count):
+            dispatch_copy(block, d).start()
+
+    def shared_hidden(block):
+        values = gath2[block]
+        gated = jnp.dot(values, sgate[...], preferred_element_type=jnp.float32)
+        lifted = jnp.dot(values, sup[...], preferred_element_type=jnp.float32)
+        hidden[block] = (jax.nn.silu(gated) * lifted).astype(jnp.bfloat16)
+
+    def expert(block):
+        for d in range(1, ep_count):
+            dispatch_copy(block, d).wait()
+
+        def units(span):
+            values = disp[block]
+            gated = jnp.dot(values, gate[:, span], preferred_element_type=jnp.float32)
+            lifted = jnp.dot(values, up[:, span], preferred_element_type=jnp.float32)
+            hexp[:, span] = (jax.nn.silu(gated) * lifted).astype(jnp.bfloat16)
+
+        spans(units, 256, gate.shape[1])
+
+        def columns(span):
+            result = jnp.dot(hexp[...], down[:, span], preferred_element_type=jnp.float32).astype(jnp.bfloat16)
+            back[block, 0:slots, span] = result[0:slots]
+            sbuf[block, slots:total, span] = result[slots:total]
+
+        spans(columns)
+        for d in range(1, ep_count):
+            return_copy(block, d).start()
+
+    def experts_at(distance):
+        def one(side, carry):
+            block = tp + (2 * side - 1) * distance
+
+            @pl.when((block >= 0) & (block < tp_count) & ((distance > 0) | (side == 0)))
+            def _():
+                expert(block)
+
+            return carry
+
+        lax.fori_loop(0, 2, one, 0)
+
+    for side in range(2):
+
+        @pl.when(exists(side))
+        def _():
+            for copy in send_second(side, tp, True):
+                copy.start()
+
+        start_own_first(side, 0)
+    for copy in own_copies + weight_copies:
+        copy.start()
+
+    @pl.when(tp == 0)
+    def _():
+        sides[0] = jnp.zeros(sides.shape[1:], sides.dtype)
+
+    @pl.when(tp == tp_count - 1)
+    def _():
+        sides[1] = jnp.zeros(sides.shape[1:], sides.dtype)
+
+    own_copies[0].wait()
+    own_copies[1].wait()
+    process(tp)
+    shared_hidden(tp)
+    for copy in weight_copies:
+        copy.wait()
+
+    def hop(k, carry):
+        for side in range(2):
+            block = tp - k if side == 0 else tp + k
+            inside = block >= 0 if side == 0 else block < tp_count
+
+            @pl.when(inside)
+            def _():
+                for copy in send_second(side, block, False):
+                    copy.wait_recv()
+
+                @pl.when(exists(side))
+                def _():
+                    for copy in send_second(side, block, False):
+                        copy.start()
+
+            start_own_first(side, k)
+
+            @pl.when(inside)
+            def _():
+                process(block)
+                shared_hidden(block)
+
+        experts_at(k - 1)
+        return carry
+
+    lax.fori_loop(1, tp_count, hop, 0)
+    own_copies[2].wait()
+
+    def partial_of(block):
+        parts = []
+        for d in range(ep_count):
+            hit, number = places_of(block, d)
+            parts.append(jnp.where(hit, metag[block, pl.ds(experts + number, 1), :], 0.0))
+        weights = jnp.concatenate(parts, axis=0)
+        high = weights.astype(jnp.bfloat16)
+        low = (weights - high.astype(jnp.float32)).astype(jnp.bfloat16)
+        turned = (((0,), (0,)), ((), ()))
+
+        def value(span):
+            picked = back[block, :, span]
+            return (
+                lax.dot_general(high, picked, turned, preferred_element_type=jnp.float32)
+                + lax.dot_general(low, picked, turned, preferred_element_type=jnp.float32)
+                + jnp.dot(hidden[block], sdown[:, span], preferred_element_type=jnp.float32)
+            )
+
+        return value
+
+    def wait_return(block):
+        for d in range(1, ep_count):
+            return_copy(block, d).wait_recv()
+
+    def reduce_step(k):
+        for side in range(2):
+            block = tp_count - 1 - k if side == 0 else k
+            active = block > tp if side == 0 else block < tp
+
+            @pl.when(active)
+            def _():
+                wait_return(block)
+
+                @pl.when(tp > 0 if side == 0 else tp < tp_count - 1)
+                def _():
+                    pass_on(side, block).wait_recv()
+
+                value = partial_of(block)
+
+                def columns(span):
+                    psend[block, :, span] = (
+                        value(span) + sides[side, block, :, span].astype(jnp.float32)
+                    ).astype(jnp.bfloat16)
+
+                spans(columns)
+                pass_on(side, block).start()
+
+    def hop_first(k, carry):
+        for side in range(2):
+            block = tp - k if side == 0 else tp + k
+            inside = block >= 0 if side == 0 else block < tp_count
+
+            @pl.when(inside)
+            def _():
+                send_first(side, block, False).wait_recv()
+
+                @pl.when(exists(side))
+                def _():
+                    send_first(side, block, False).start()
+
+        @pl.when(k == 1)
+        def _():
+            experts_at(tp_count - 1)
+
+        @pl.when(k > 1)
+        def _():
+            reduce_step(k - 2)
+
+        return carry
+
+    lax.fori_loop(1, tp_count, hop_first, 0)
+    reduce_step(tp_count - 2)
+    wait_return(tp)
+
+    @pl.when(tp > 0)
+    def _():
+        pass_on(0, tp).wait_recv()
+
+    @pl.when(tp < tp_count - 1)
+    def _():
+        pass_on(1, tp).wait_recv()
+
+    own_value = partial_of(tp)
+
+    def columns(span):
+        out[:, span] = (
+            own_value(span)
+            + sides[0, tp, :, span].astype(jnp.float32)
+            + sides[1, tp, :, span].astype(jnp.float32)
+        ).astype(jnp.bfloat16)
+
+    spans(columns)
+
+    def finish(block, carry):
+        for d in range(1, ep_count):
+            return_copy(block, d).wait_send()
+        for side in range(2):
+            passed = block <= tp if side == 0 else block >= tp
+            summed = block > tp if side == 0 else block < tp
+
+            @pl.when(exists(side) & passed)
+            def _():
+                for copy in send_second(side, block, False):
+                    copy.wait_send()
+                send_first(side, block, False).wait_send()
+
+            @pl.when(summed)
+            def _():
+                pass_on(side, block).wait_send()
+
+        return carry
+
+    lax.fori_loop(0, tp_count, finish, 0)
+
+
+def layer(second, first, meta, gate, up, down, sgate, sup, sdown, ep_count, tp_count, slots):
+    rows, width = second.shape
+    vmem = pl.BlockSpec(memory_space=pltpu.VMEM)
+    hbm = pl.BlockSpec(memory_space=pl.ANY)
+    dma = pltpu.SemaphoreType.DMA
+    bf16 = jnp.bfloat16
+    total = ep_count * slots
+    return pl.pallas_call(
+        functools.partial(layer_kernel, ep_count, tp_count, slots),
+        out_shape=(
+            jax.ShapeDtypeStruct((rows, width), bf16),
+            jax.ShapeDtypeStruct((tp_count, rows, width), bf16),
+        ),
+        in_specs=[vmem] * 3 + [hbm] * 3 + [vmem] * 3,
+        out_specs=(vmem, vmem),
+        scratch_shapes=[
+            pltpu.VMEM((tp_count, rows, width), bf16),
+            pltpu.VMEM((tp_count,) + meta.shape, jnp.float32),
+            pltpu.VMEM((tp_count, total, width), bf16),
+            pltpu.VMEM((tp_count, total, width), bf16),
+            pltpu.VMEM((tp_count, total, width), bf16),
+            pltpu.VMEM((2, tp_count, rows, width), bf16),
+            pltpu.VMEM((tp_count, rows, width), bf16),
+            pltpu.VMEM(gate.shape[1:], bf16),
+            pltpu.VMEM(up.shape[1:], bf16),
+            pltpu.VMEM(down.shape[1:], bf16),
+            pltpu.VMEM((tp_count, rows, sgate.shape[1]), bf16),
+            pltpu.VMEM((total, gate.shape[2]), bf16),
+            dma((3,)),
+            dma((3,)),
+            dma((2, tp_count)),
+            dma((tp_count,)),
+            dma((2, tp_count)),
+            dma((tp_count,)),
+            dma((2, tp_count)),
+            dma((tp_count,)),
+            dma((tp_count, ep_count)),
+            dma((tp_count, ep_count)),
+            dma((tp_count, ep_count)),
+            dma((tp_count, ep_count)),
+            dma((tp_count,)),
+            dma((2, tp_count)),
+        ],
+        compiler_params=pltpu.CompilerParams(
+            collective_id=0, has_side_effects=True, vmem_limit_bytes=VMEM_LIMIT
+        ),
+        name="layer",
+    )(second, first, meta, gate, up, down, sgate, sup, sdown)
+
+
 def body(
     mixer_in,
     mixer_gain,
@@ -105,30 +487,38 @@
     shared_up,
     shared_down,
 ):
+    tokens = mixer_in.shape[0]
+    ep_count, tp_count = lax.axis_size("ep"), lax.axis_size("tp")
+    top_count = routes.shape[1]
+    experts = router.shape[1]
+    capacity = 3 * top_count * tokens // (2 * experts)
+    slots = -(-capacity // 16) * 16
+    normed_second = rms_rows(moe_in, moe_gain)
     normed_first = rms_rows(mixer_in, mixer_gain)
-    normed_second = rms_rows(moe_in, moe_gain)
+    affinity = jax.nn.sigmoid(jnp.dot(normed_second, router, preferred_element_type=jnp.float32))
+    hits = jnp.any(
+        routes[:, :, None] == jnp.arange(experts, dtype=jnp.int32)[None, None, :], axis=1
+    )
+    chosen = jnp.where(hits, affinity, 0.0)
+    route_weight = ROUTED_SCALE * chosen / jnp.sum(chosen, axis=-1, keepdims=True)
+    earlier = jnp.tril(jnp.ones((tokens, tokens), jnp.bfloat16), -1)
+    before = jnp.dot(earlier, hits.astype(jnp.bfloat16), preferred_element_type=jnp.float32)
+    places = jnp.where(hits, before, -1.0)
+    meta = jnp.concatenate([places, route_weight], axis=1).T
+    width = normed_second.shape[1]
+    moe_out, gathered_first = layer(
+        normed_second, normed_first, meta, expert_gate, expert_up, expert_down,
+        shared_gate, shared_up, shared_down, ep_count, tp_count, slots,
+    )
     query_cols = w_query.shape[1]
     key_cols = w_key.shape[1]
     joined = jnp.concatenate([w_query, w_key, w_value], axis=1)
-    gathered_first, gathered_second = (
-        lax.all_gather(normed_first, "tp", axis=0, tiled=True),
-        lax.all_gather(normed_second, "tp", axis=0, tiled=True),
-    )
-    projected = jnp.dot(gathered_first, joined, preferred_element_type=jnp.float32)
-    row_block = gathered_second
-    hidden = (
-        jax.nn.silu(jnp.dot(row_block, shared_gate, preferred_element_type=jnp.float32))
-        * jnp.dot(row_block, shared_up, preferred_element_type=jnp.float32)
-    ).astype(jnp.bfloat16)
-    shared = lax.psum_scatter(
-        jnp.dot(hidden, shared_down, preferred_element_type=jnp.float32),
-        "tp",
-        scatter_dimension=0,
-        tiled=True,
+    projected = jnp.dot(
+        gathered_first.reshape(-1, width), joined, preferred_element_type=jnp.float32
     )
     span_rows = projected.shape[0]
     offset = lax.axis_index("ep") * span_rows
-    seq_length = span_rows * lax.axis_size("ep")
+    seq_length = span_rows * ep_count
     positions = offset + jnp.arange(span_rows, dtype=jnp.int32)
     query_rows = rotate(
         projected[:, :query_cols].reshape(span_rows, -1, HEAD_DIM), positions
@@ -140,43 +530,6 @@
     stacked = jnp.concatenate([key_rows.reshape(span_rows, key_cols), value_rows], axis=1)
     padded = extended(stacked, (("ep", 0),), WINDOW)
     mixed = attend(query_rows, padded, sink_logit, offset, seq_length)
-    tokens = normed_second.shape[0]
-    top_count = routes.shape[1]
-    experts = router.shape[1]
-    capacity = 3 * top_count * tokens // (2 * experts)
-    affinity = jax.nn.sigmoid(jnp.dot(normed_second, router, preferred_element_type=jnp.float32))
-    hit_table = routes[:, :, None] == jnp.arange(experts, dtype=jnp.int32)[None, None, :]
-    chosen = jnp.sum(jnp.where(hit_table, affinity[:, None, :], 0.0), axis=-1)
-    route_weight = ROUTED_SCALE * chosen / jnp.sum(chosen, axis=-1, keepdims=True)
-    flat_hits = hit_table.reshape(tokens * top_count, experts).astype(jnp.int32)
-    slot_index = jnp.sum((jnp.cumsum(flat_hits, axis=0) - 1) * flat_hits, axis=-1)
-    target = routes.reshape(-1) * capacity + slot_index
-    source = jnp.arange(tokens * top_count, dtype=jnp.int32) // top_count
-    outgoing = (
-        jnp.zeros((experts * capacity, normed_second.shape[1]), jnp.bfloat16)
-        .at[target]
-        .set(normed_second[source])
-    )
-    outgoing = outgoing.reshape(experts, capacity, -1)
-    row_block = lax.all_to_all(outgoing, ("ep", "tp"), split_axis=0, concat_axis=0, tiled=True)
-    row_shape = row_block.shape
-    flat_rows = row_block.reshape(-1, row_shape[-1])
-    hidden_rows = (
-        jax.nn.silu(jnp.dot(flat_rows, expert_gate[0], preferred_element_type=jnp.float32))
-        * jnp.dot(flat_rows, expert_up[0], preferred_element_type=jnp.float32)
-    ).astype(jnp.bfloat16)
-    returned = lax.all_to_all(
-        jnp.dot(hidden_rows, expert_down[0], preferred_element_type=jnp.float32)
-        .astype(jnp.bfloat16)
-        .reshape(row_shape),
-        ("ep", "tp"),
-        split_axis=0,
-        concat_axis=0,
-        tiled=True,
-    )
-    picked = returned.reshape(experts * capacity, -1)[target].reshape(tokens, top_count, -1)
-    routed = jnp.sum(picked.astype(jnp.float32) * route_weight[:, :, None], axis=1)
-    moe_out = (routed + shared).astype(jnp.bfloat16)
     return (mixed, moe_out)
 
 

time: 333 us -> 155 us (0.47)
  waiting for transfers between devices: 226 us -> 0.1 us
  Pallas kernels: 0 us -> 119 us
  local copies, waits for them, and re-layouts: 26.3 us -> 1.85 us
  matrix products: 29.4 us -> 7.21 us
  between operations: 14 us -> 0.84 us
  other arithmetic: 16.3 us -> 8.89 us
    all_to_all x2 -> x0, waiting for transfers between devices: 161 us -> none  [the longest x1 105 us: body(): lax.all_to_all(jnp.dot(hidden_rows, expert_down[0], preferred_element_typ...]
    pallas_call x0 -> x1, Pallas kernels: none -> 119 us  [layer(): pl.pallas_call(functools.partial(layer_kernel, ep_count, tp_count, slots)...]
    all_gather x2 -> x0, waiting for transfers between devices: 60.4 us -> none  [the longest x1 60.4 us: body(): lax.all_gather(normed_second, 'tp', axis=0, tiled=True)]
    dot_general x5 -> x2, matrix products: 25.9 us -> 3.67 us  [the longest x1 3.47 us: body(): jnp.dot(gathered_first.reshape(-1, width), joined, preferred_element_type...]
    all_to_all x2 -> x0, starting transfers between devices: 13.3 us -> none  [the longest x1 7.47 us: body(): lax.all_to_all(outgoing, ('ep', 'tp'), split_axis=0, concat_axis=0, tiled...]
    ppermute x1, starting transfers between devices: 2.14 us -> 14.4 us  [extended(): lax.ppermute(lax.slice_in_dim(block, 0, width, axis=dim), axis, backward)]
    scatter x1 -> x0, local copies, waits for them, and re-layouts: 12.1 us -> none  [body(): outgoing = jnp.zeros((experts * capacity, normed_second.shape[1]), jnp.bf...]
    gather x1 -> x0, local copies, waits for them, and re-layouts: 7.52 us -> none  [body(): returned.reshape(experts * capacity, -1)[target]]
  transfers between devices with their start and end apart: 7 -> 2, of which waited for: 5 -> 1; matrix products, arithmetic and copies ran while one was open for 20% -> 1% of each run, Pallas kernels for 0% -> 0%
where the time goes in v2:
time: 155 us
  Pallas kernels  119 us (77%)
  starting transfers between devices  16.6 us (11%)
  other arithmetic  8.89 us (6%)
  matrix products  7.21 us (5%)
  local copies, waits for them, and re-layouts  1.85 us (1%)
    pallas_call x1, Pallas kernels, layer(): pl.pallas_call(functools.partial(layer_kernel, ep_count, tp_count, slots)...  119 us
    ppermute x1, starting transfers between devices, extended(): lax.ppermute(lax.slice_in_dim(block, 0, width, axis=dim), axis, backward)  14.4 us
    dot_general x1, matrix products, body(): jnp.dot(gathered_first.reshape(-1, width), joined, preferred_element_type...  3.47 us
  transfers between devices with their start and end apart: 2, of which 1 were waited for; matrix products, arithmetic and copies ran while one was open for 1% of the time, Pallas kernels for 0%

profile of v2, /device:TPU:1, one launch (start us, length us, event | category | flops | bytes accessed | tf_op | source)
XLA Modules:
  0.0 154.5 jit_solution(7332889279996729578)
XLA Ops:
  0.6 0.0 copy-start
  0.7 1.3 fusion.16
  1.9 1.2 fusion.19
  3.2 0.7 fusion.29
  3.9 0.2 convolution_select_fusion
  4.1 2.2 %fusion.18 = (bf16[128,2048]{1,0:T(8,128)(2,1)S(1)}, bf16[128,2048]{1,0:T(8,128)(2,1)}) fusion(bf16[128,2048]{1,0:T(8,128)(2,1)} %param.22, f32[2048]{0:T(1024)} %param.23, f32[128]{0:T(128)S(1)} %add_rsqrt_fusion.1, f32[2048]{0:T(1024)} %param.17, f32[128]{0:T(128)S(1)} %add_rsqrt_fusion, bf16[128,2048]{1,0:T(8,128)(2,1)} %param.16), kind=kLoop, calls=%fused_computation.28 | loop fusion | flops 2097152 | bytes 2114560 | tf_op jit(solution)/shard_map/convert_element_type | solution.py:35
  6.3 0.0 copy-start.1
  6.3 0.0 copy-done
  6.3 0.3 fusion.42
  6.6 0.6 maximum_bitcast_fusion.meta
  7.2 0.0 copy-done.1
  7.2 119.0 %layer.1 = (bf16[128,2048]{1,0:T(8,128)(2,1)}, bf16[4,128,2048]{2,1,0:T(8,128)(2,1)}) custom-call(bf16[128,2048]{1,0:T(8,128)(2,1)} %copy-done.1, bf16[128,2048]{1,0:T(8,128)(2,1)} %get-tuple-element.52.first, f32[32,128]{1,0:T(8,128)} %maximum_bitcast_fusion.meta, bf16[1,2048,512]{2,1,0:T(8,128)(2,1)} %gate_hbm.1, bf16[1,2048,512]{2,1,0:T(8,128)(2,1)} %up_hbm.1, ...), custom_call_target="tpu_custom_call" | custom-call | tf_op jit(solution)/shard_map/layer/pallas_call | solution.py:429
  126.3 3.5 %fusion.3 = f32[512,512]{0,1:T(8,128)S(1)} fusion(bf16[512,2048]{1,0:T(8,128)(2,1)} %bitcast.47, bf16[2048,128]{1,0:T(8,128)(2,1)} %param.20, bf16[2048,128]{1,0:T(8,128)(2,1)} %param.19, bf16[2048,256]{1,0:T(8,128)(2,1)} %param.18), kind=kOutput, calls=%fused_computation.6 | convolution fusion | flops 1080033280 | bytes 5242880 | tf_op jit(solution)/shard_map/dot_general | solution.py:516
  129.7 0.0 copy-start.3
  129.8 0.3 multiply_cosine_fusion
  130.2 14.4 %collective-permute-start.1 = (bf16[128,256]{0,1:T(8,128)(2,1)S(1)}, bf16[128,256]{0,1:T(8,128)(2,1)S(1)}, u32[]{:S(2)}, u32[]{:S(2)}) collective-permute-start(bf16[128,256]{0,1:T(8,128)(2,1)S(1)} %get-tuple-element.44), channel_id=1, source_target_pairs={{4,0},{8,4},{12,8},{5,1},{9,5},{13,9},{6,2},{10,6},{14,10},{7,3},{... | collective-permute-start | bytes 196616 | tf_op jit(solution)/shard_map/ppermute | solution.py:27
  144.7 2.2 %collective-permute-start = (bf16[128,256]{0,1:T(8,128)(2,1)S(1)}, bf16[128,256]{0,1:T(8,128)(2,1)S(1)}, u32[]{:S(2)}, u32[]{:S(2)}) collective-permute-start(bf16[128,256]{0,1:T(8,128)(2,1)S(1)} %get-tuple-element.43), channel_id=1, source_target_pairs={{0,4},{4,8},{8,12},{1,5},{5,9},{9,13},{2,6},{6,10},{10,14},{3,7},{... | collective-permute-start | bytes 196616 | tf_op jit(solution)/shard_map/ppermute | solution.py:24
  146.9 0.1 subtract_convert_fusion
  147.0 0.8 fusion.10
  147.8 0.0 copy-done.3
  147.8 0.1 max.22
  147.9 0.0 collective-permute-done.1
  147.9 0.1 collective-permute-done
  148.0 1.3 fusion.1
  149.3 0.1 broadcast_maximum_fusion
  149.4 1.4 fusion
  150.8 0.1 exponential_add_fusion
  150.9 0.0 copy-start.2
  150.9 2.0 %fusion.11 = bf16[2,64,2,512]{3,1,2,0:T(8,128)(2,1)S(1)} fusion(bf16[768,2,64,1]{0,2,3,1:T(8,128)(2,1)S(1)} %bitcast.43, f32[2,768,512,2]{2,1,3,0:T(8,128)S(1)} %get-tuple-element.50, f32[2,2,512]{2,1,0:T(2,128)S(1)} %exponential_add_fusion, f32[2,2,512]{2,1,0:T(2,128)S(1)} %broadcast_maximum_fusion, pred[512,768]{0,1:T(8,128)(4,1)S(1)} %fusion.10), kind=kOutput, calls=%fused_computation.19 | convolution fusion | flops 209321984 | bytes 7159808 | tf_op jit(solution)/shard_map/while/body/eval_jaxpr/kgqc,ckd->qkgd/dot_general | solution.py:85
  152.9 0.8 copy.22
  153.7 0.0 copy-done.2
  153.7 0.8 copy.27
  (16 shorter events, 0.3 us)
Async XLA Ops:
  0.6 5.7 %copy-start = (bf16[2048,16]{0,1:T(8,128)(2,1)S(1)}, bf16[2048,16]{0,1:T(8,128)(2,1)}, u32[]{:S(2)}) copy-start(bf16[2048,16]{0,1:T(8,128)(2,1)} %param.24) | copy-start | bytes 196612
  6.3 0.9 copy-start.1
  129.7 18.0 %copy-start.3 = (f32[4]{0:T(128)S(1)}, f32[4]{0:T(128)}, u32[]{:S(2)}) copy-start(f32[4]{0:T(128)} %param.21) | copy-start | bytes 52
  130.2 17.6 %collective-permute-start.1 = (bf16[128,256]{0,1:T(8,128)(2,1)S(1)}, bf16[128,256]{0,1:T(8,128)(2,1)S(1)}, u32[]{:S(2)}, u32[]{:S(2)}) collective-permute-start(bf16[128,256]{0,1:T(8,128)(2,1)S(1)} %get-tuple-element.44), channel_id=1, source_target_pairs={{4,0},{8,4},{12,8},{5,1},{9,5},{13,9},{6,2},{10,6},{14,10},{7,3},{... | collective-permute-start | bytes 196616 | tf_op jit(solution)/shard_map/ppermute | solution.py:27
  144.7 3.3 %collective-permute-start = (bf16[128,256]{0,1:T(8,128)(2,1)S(1)}, bf16[128,256]{0,1:T(8,128)(2,1)S(1)}, u32[]{:S(2)}, u32[]{:S(2)}) collective-permute-start(bf16[128,256]{0,1:T(8,128)(2,1)S(1)} %get-tuple-element.43), channel_id=1, source_target_pairs={{0,4},{4,8},{8,12},{1,5},{5,9},{9,13},{2,6},{6,10},{10,14},{3,7},{... | collective-permute-start | bytes 196616 | tf_op jit(solution)/shard_map/ppermute | solution.py:24
  150.9 2.9 %copy-start.2 = (bf16[128,2048]{1,0:T(8,128)(2,1)S(1)}, bf16[128,2048]{1,0:T(8,128)(2,1)}, u32[]{:S(2)}) copy-start(bf16[128,2048]{1,0:T(8,128)(2,1)} %get-tuple-element.60) | copy-start | bytes 1572868

commit v3 on v2

--- a/solution.py
+++ b/solution.py
@@ -190,8 +190,17 @@
         part = pl.ds(d * slots, slots)
         return remote(sbuf.at[block, part], back.at[block, part], sb.at[block, d], rb.at[block, d], peer(ep_count - d))
 
-    def pass_on(side, block):
-        return remote(psend.at[block], sides.at[side, block], sp.at[block], rs.at[side, block], toward(side))
+    parts = width // CHUNK
+
+    def part_span(part):
+        return pl.ds(pl.multiple_of(part * CHUNK, CHUNK), CHUNK)
+
+    def pass_on(side, block, part):
+        span = part_span(part)
+        return remote(
+            psend.at[block, :, span], sides.at[side, block, :, span],
+            sp.at[block, part], rs.at[side, block, part], toward(side),
+        )
 
     def places_of(block, d):
         expert = lax.rem(ep + d, ep_count) * tp_count + tp
@@ -305,11 +314,11 @@
     own_copies[2].wait()
 
     def partial_of(block):
-        parts = []
+        pieces = []
         for d in range(ep_count):
             hit, number = places_of(block, d)
-            parts.append(jnp.where(hit, metag[block, pl.ds(experts + number, 1), :], 0.0))
-        weights = jnp.concatenate(parts, axis=0)
+            pieces.append(jnp.where(hit, metag[block, pl.ds(experts + number, 1), :], 0.0))
+        weights = jnp.concatenate(pieces, axis=0)
         high = weights.astype(jnp.bfloat16)
         low = (weights - high.astype(jnp.float32)).astype(jnp.bfloat16)
         turned = (((0,), (0,)), ((), ()))
@@ -328,28 +337,31 @@
         for d in range(1, ep_count):
             return_copy(block, d).wait_recv()
 
-    def reduce_step(k):
+    def reduce_step(step):
         for side in range(2):
-            block = tp_count - 1 - k if side == 0 else k
-            active = block > tp if side == 0 else block < tp
+            block = step - tp if side == 0 else 2 * (tp_count - 1) - step - tp
+            active = (block > tp) & (block < tp_count) if side == 0 else (block < tp) & (block >= 0)
 
             @pl.when(active)
             def _():
                 wait_return(block)
-
-                @pl.when(tp > 0 if side == 0 else tp < tp_count - 1)
-                def _():
-                    pass_on(side, block).wait_recv()
-
                 value = partial_of(block)
 
-                def columns(span):
+                def one_part(part, carry):
+                    span = part_span(part)
+                    own = value(span)
+
+                    @pl.when(tp > 0 if side == 0 else tp < tp_count - 1)
+                    def _():
+                        pass_on(side, block, part).wait_recv()
+
                     psend[block, :, span] = (
-                        value(span) + sides[side, block, :, span].astype(jnp.float32)
+                        own + sides[side, block, :, span].astype(jnp.float32)
                     ).astype(jnp.bfloat16)
-
-                spans(columns)
-                pass_on(side, block).start()
+                    pass_on(side, block, part).start()
+                    return carry
+
+                lax.fori_loop(0, parts, one_part, 0)
 
     def hop_first(k, carry):
         for side in range(2):
@@ -368,34 +380,34 @@
         def _():
             experts_at(tp_count - 1)
 
-        @pl.when(k > 1)
+        reduce_step(2 * k - 1)
+        reduce_step(2 * k)
+        return carry
+
+    lax.fori_loop(1, tp_count, hop_first, 0)
+    wait_return(tp)
+    own_value = partial_of(tp)
+
+    def last_part(part, carry):
+        span = part_span(part)
+        own = own_value(span)
+
+        @pl.when(tp > 0)
         def _():
-            reduce_step(k - 2)
-
-        return carry
-
-    lax.fori_loop(1, tp_count, hop_first, 0)
-    reduce_step(tp_count - 2)
-    wait_return(tp)
-
-    @pl.when(tp > 0)
-    def _():
-        pass_on(0, tp).wait_recv()
-
-    @pl.when(tp < tp_count - 1)
-    def _():
-        pass_on(1, tp).wait_recv()
-
-    own_value = partial_of(tp)
-
-    def columns(span):
+            pass_on(0, tp, part).wait_recv()
+
+        @pl.when(tp < tp_count - 1)
+        def _():
+            pass_on(1, tp, part).wait_recv()
+
         out[:, span] = (
-            own_value(span)
+            own
             + sides[0, tp, :, span].astype(jnp.float32)
             + sides[1, tp, :, span].astype(jnp.float32)
         ).astype(jnp.bfloat16)
-
-    spans(columns)
+        return carry
+
+    lax.fori_loop(0, parts, last_part, 0)
 
     def finish(block, carry):
         for d in range(1, ep_count):
@@ -412,7 +424,8 @@
 
             @pl.when(summed)
             def _():
-                pass_on(side, block).wait_send()
+                for part in range(parts):
+                    pass_on(side, block, part).wait_send()
 
         return carry
 
@@ -459,8 +472,8 @@
             dma((tp_count, ep_count)),
             dma((tp_count, ep_count)),
             dma((tp_count, ep_count)),
-            dma((tp_count,)),
-            dma((2, tp_count)),
+            dma((tp_count, width // CHUNK)),
+            dma((2, tp_count, width // CHUNK)),
         ],
         compiler_params=pltpu.CompilerParams(
             collective_id=0, has_side_effects=True, vmem_limit_bytes=VMEM_LIMIT

time: 155 us -> 142 us (0.916)
  starting transfers between devices: 16.6 us -> 5.74 us
  Pallas kernels: 119 us -> 117 us
    ppermute x1, starting transfers between devices: 14.4 us -> 2.26 us  [extended(): lax.ppermute(lax.slice_in_dim(block, 0, width, axis=dim), axis, backward)]
    pallas_call x1, Pallas kernels: 119 us -> 117 us  [layer(): pl.pallas_call(functools.partial(layer_kernel, ep_count, tp_count, slots)...]
where the time goes in v3:
time: 142 us
  Pallas kernels  117 us (82%)
  other arithmetic  8.89 us (6%)
  matrix products  7.21 us (5%)
  starting transfers between devices  5.74 us (4%)
  local copies, waits for them, and re-layouts  1.85 us (1%)
    pallas_call x1, Pallas kernels, layer(): pl.pallas_call(functools.partial(layer_kernel, ep_count, tp_count, slots)...  117 us
    ppermute x1, starting transfers between devices, extended(): lax.ppermute(lax.slice_in_dim(block, block.shape[dim] - width, None, axis...  3.48 us
    dot_general x1, matrix products, body(): jnp.dot(gathered_first.reshape(-1, width), joined, preferred_element_type...  3.47 us
  transfers between devices with their start and end apart: 2, of which 1 were waited for; matrix products, arithmetic and copies ran while one was open for 1% of the time, Pallas kernels for 0%

profile of v3, /device:TPU:1, one launch (start us, length us, event | category | flops | bytes accessed | tf_op | source)
XLA Modules:
  0.0 142.0 jit_solution(77101463712454393)
XLA Ops:
  0.6 0.0 copy-start
  0.7 1.3 fusion.16
  1.9 1.2 fusion.19
  3.2 0.7 fusion.29
  3.9 0.2 convolution_select_fusion
  4.1 2.2 %fusion.18 = (bf16[128,2048]{1,0:T(8,128)(2,1)S(1)}, bf16[128,2048]{1,0:T(8,128)(2,1)}) fusion(bf16[128,2048]{1,0:T(8,128)(2,1)} %param.22, f32[2048]{0:T(1024)} %param.23, f32[128]{0:T(128)S(1)} %add_rsqrt_fusion.1, f32[2048]{0:T(1024)} %param.17, f32[128]{0:T(128)S(1)} %add_rsqrt_fusion, bf16[128,2048]{1,0:T(8,128)(2,1)} %param.16), kind=kLoop, calls=%fused_computation.28 | loop fusion | flops 2097152 | bytes 2114560 | tf_op jit(solution)/shard_map/convert_element_type | solution.py:35
  6.3 0.0 copy-start.1
  6.3 0.0 copy-done
  6.3 0.3 fusion.42
  6.6 0.6 maximum_bitcast_fusion.meta
  7.2 0.0 copy-done.1
  7.2 117.4 %layer.1 = (bf16[128,2048]{1,0:T(8,128)(2,1)}, bf16[4,128,2048]{2,1,0:T(8,128)(2,1)}) custom-call(bf16[128,2048]{1,0:T(8,128)(2,1)} %copy-done.1, bf16[128,2048]{1,0:T(8,128)(2,1)} %get-tuple-element.52.first, f32[32,128]{1,0:T(8,128)} %maximum_bitcast_fusion.meta, bf16[1,2048,512]{2,1,0:T(8,128)(2,1)} %gate_hbm.1, bf16[1,2048,512]{2,1,0:T(8,128)(2,1)} %up_hbm.1, ...), custom_call_target="tpu_custom_call" | custom-call | tf_op jit(solution)/shard_map/layer/pallas_call | solution.py:442
  124.6 3.5 %fusion.3 = f32[512,512]{0,1:T(8,128)S(1)} fusion(bf16[512,2048]{1,0:T(8,128)(2,1)} %bitcast.47, bf16[2048,128]{1,0:T(8,128)(2,1)} %param.20, bf16[2048,128]{1,0:T(8,128)(2,1)} %param.19, bf16[2048,256]{1,0:T(8,128)(2,1)} %param.18), kind=kOutput, calls=%fused_computation.6 | convolution fusion | flops 1080033280 | bytes 5242880 | tf_op jit(solution)/shard_map/dot_general | solution.py:529
  128.1 0.0 copy-start.3
  128.2 0.3 multiply_cosine_fusion
  128.6 2.3 %collective-permute-start.1 = (bf16[128,256]{0,1:T(8,128)(2,1)S(1)}, bf16[128,256]{0,1:T(8,128)(2,1)S(1)}, u32[]{:S(2)}, u32[]{:S(2)}) collective-permute-start(bf16[128,256]{0,1:T(8,128)(2,1)S(1)} %get-tuple-element.44), channel_id=1, source_target_pairs={{4,0},{8,4},{12,8},{5,1},{9,5},{13,9},{6,2},{10,6},{14,10},{7,3},{... | collective-permute-start | bytes 196616 | tf_op jit(solution)/shard_map/ppermute | solution.py:27
  130.9 3.5 %collective-permute-start = (bf16[128,256]{0,1:T(8,128)(2,1)S(1)}, bf16[128,256]{0,1:T(8,128)(2,1)S(1)}, u32[]{:S(2)}, u32[]{:S(2)}) collective-permute-start(bf16[128,256]{0,1:T(8,128)(2,1)S(1)} %get-tuple-element.43), channel_id=1, source_target_pairs={{0,4},{4,8},{8,12},{1,5},{5,9},{9,13},{2,6},{6,10},{10,14},{3,7},{... | collective-permute-start | bytes 196616 | tf_op jit(solution)/shard_map/ppermute | solution.py:24
  134.4 0.1 subtract_convert_fusion
  134.5 0.8 fusion.10
  135.3 0.0 copy-done.3
  135.3 0.1 max.22
  135.4 0.0 collective-permute-done.1
  135.4 0.1 collective-permute-done
  135.6 1.3 fusion.1
  136.8 0.1 broadcast_maximum_fusion
  136.9 1.4 fusion
  138.3 0.1 exponential_add_fusion
  138.4 0.0 copy-start.2
  138.4 2.0 %fusion.11 = bf16[2,64,2,512]{3,1,2,0:T(8,128)(2,1)S(1)} fusion(bf16[768,2,64,1]{0,2,3,1:T(8,128)(2,1)S(1)} %bitcast.43, f32[2,768,512,2]{2,1,3,0:T(8,128)S(1)} %get-tuple-element.50, f32[2,2,512]{2,1,0:T(2,128)S(1)} %exponential_add_fusion, f32[2,2,512]{2,1,0:T(2,128)S(1)} %broadcast_maximum_fusion, pred[512,768]{0,1:T(8,128)(4,1)S(1)} %fusion.10), kind=kOutput, calls=%fused_computation.19 | convolution fusion | flops 209321984 | bytes 7159808 | tf_op jit(solution)/shard_map/while/body/eval_jaxpr/kgqc,ckd->qkgd/dot_general | solution.py:85
  140.4 0.8 copy.22
  141.2 0.0 copy-done.2
  141.2 0.8 copy.27
  (16 shorter events, 0.3 us)
Async XLA Ops:
  0.6 5.7 %copy-start = (bf16[2048,16]{0,1:T(8,128)(2,1)S(1)}, bf16[2048,16]{0,1:T(8,128)(2,1)}, u32[]{:S(2)}) copy-start(bf16[2048,16]{0,1:T(8,128)(2,1)} %param.24) | copy-start | bytes 196612
  6.3 0.9 copy-start.1
  128.1 7.2 %copy-start.3 = (f32[4]{0:T(128)S(1)}, f32[4]{0:T(128)}, u32[]{:S(2)}) copy-start(f32[4]{0:T(128)} %param.21) | copy-start | bytes 52
  128.6 6.8 %collective-permute-start.1 = (bf16[128,256]{0,1:T(8,128)(2,1)S(1)}, bf16[128,256]{0,1:T(8,128)(2,1)S(1)}, u32[]{:S(2)}, u32[]{:S(2)}) collective-permute-start(bf16[128,256]{0,1:T(8,128)(2,1)S(1)} %get-tuple-element.44), channel_id=1, source_target_pairs={{4,0},{8,4},{12,8},{5,1},{9,5},{13,9},{6,2},{10,6},{14,10},{7,3},{... | collective-permute-start | bytes 196616 | tf_op jit(solution)/shard_map/ppermute | solution.py:27
  130.9 4.6 %collective-permute-start = (bf16[128,256]{0,1:T(8,128)(2,1)S(1)}, bf16[128,256]{0,1:T(8,128)(2,1)S(1)}, u32[]{:S(2)}, u32[]{:S(2)}) collective-permute-start(bf16[128,256]{0,1:T(8,128)(2,1)S(1)} %get-tuple-element.43), channel_id=1, source_target_pairs={{0,4},{4,8},{8,12},{1,5},{5,9},{9,13},{2,6},{6,10},{10,14},{3,7},{... | collective-permute-start | bytes 196616 | tf_op jit(solution)/shard_map/ppermute | solution.py:24
  138.4 2.9 %copy-start.2 = (bf16[128,2048]{1,0:T(8,128)(2,1)S(1)}, bf16[128,2048]{1,0:T(8,128)(2,1)}, u32[]{:S(2)}) copy-start(bf16[128,2048]{1,0:T(8,128)(2,1)} %get-tuple-element.60) | copy-start | bytes 1572868

commit v4 on v3

--- a/solution.py
+++ b/solution.py
@@ -244,6 +244,8 @@
             sbuf[block, slots:total, span] = result[slots:total]
 
         spans(columns)
+
+    def give_back(block):
         for d in range(1, ep_count):
             return_copy(block, d).start()
 
@@ -254,6 +256,10 @@
             @pl.when((block >= 0) & (block < tp_count) & ((distance > 0) | (side == 0)))
             def _():
                 expert(block)
+
+                @pl.when(block != tp)
+                def _():
+                    give_back(block)
 
             return carry
 
@@ -379,6 +385,7 @@
         @pl.when(k == 1)
         def _():
             experts_at(tp_count - 1)
+            give_back(tp)
 
         reduce_step(2 * k - 1)
         reduce_step(2 * k)

time: 142 us -> 140 us (0.986)
  Pallas kernels: 117 us -> 115 us
    pallas_call x1, Pallas kernels: 117 us -> 115 us  [layer(): pl.pallas_call(functools.partial(layer_kernel, ep_count, tp_count, slots)...]
where the time goes in v4:
time: 140 us; the launch traced here: 139 us
  Pallas kernels  115 us (82%)
  other arithmetic  8.89 us (6%)
  matrix products  7.21 us (5%)
  starting transfers between devices  5.74 us (4%)
  local copies, waits for them, and re-layouts  1.85 us (1%)
    pallas_call x1, Pallas kernels, layer(): pl.pallas_call(functools.partial(layer_kernel, ep_count, tp_count, slots)...  115 us
    dot_general x1, matrix products, body(): jnp.dot(gathered_first.reshape(-1, width), joined, preferred_element_type...  3.47 us
    ppermute x1, starting transfers between devices, extended(): lax.ppermute(lax.slice_in_dim(block, block.shape[dim] - width, None, axis...  2.89 us
    ppermute x1, starting transfers between devices, extended(): lax.ppermute(lax.slice_in_dim(block, 0, width, axis=dim), axis, backward)  2.85 us
  transfers between devices with their start and end apart: 2, of which 1 were waited for; matrix products, arithmetic and copies ran while one was open for 1% of the time, Pallas kernels for 0%

profile of v4, /device:TPU:1, one launch (start us, length us, event | category | flops | bytes accessed | tf_op | source)
XLA Modules:
  0.0 139.3 jit_solution(12043619239715672302)
XLA Ops:
  0.6 0.0 copy-start
  0.7 1.3 fusion.16
  1.9 1.2 fusion.19
  3.2 0.7 fusion.29
  3.9 0.2 convolution_select_fusion
  4.1 2.2 %fusion.18 = (bf16[128,2048]{1,0:T(8,128)(2,1)S(1)}, bf16[128,2048]{1,0:T(8,128)(2,1)}) fusion(bf16[128,2048]{1,0:T(8,128)(2,1)} %param.22, f32[2048]{0:T(1024)} %param.23, f32[128]{0:T(128)S(1)} %add_rsqrt_fusion.1, f32[2048]{0:T(1024)} %param.17, f32[128]{0:T(128)S(1)} %add_rsqrt_fusion, bf16[128,2048]{1,0:T(8,128)(2,1)} %param.16), kind=kLoop, calls=%fused_computation.28 | loop fusion | flops 2097152 | bytes 2114560 | tf_op jit(solution)/shard_map/convert_element_type | solution.py:35
  6.3 0.0 copy-start.1
  6.3 0.0 copy-done
  6.3 0.3 fusion.42
  6.6 0.6 maximum_bitcast_fusion.meta
  7.2 0.0 copy-done.1
  7.2 114.6 %layer.1 = (bf16[128,2048]{1,0:T(8,128)(2,1)}, bf16[4,128,2048]{2,1,0:T(8,128)(2,1)}) custom-call(bf16[128,2048]{1,0:T(8,128)(2,1)} %copy-done.1, bf16[128,2048]{1,0:T(8,128)(2,1)} %get-tuple-element.52.first, f32[32,128]{1,0:T(8,128)} %maximum_bitcast_fusion.meta, bf16[1,2048,512]{2,1,0:T(8,128)(2,1)} %gate_hbm.1, bf16[1,2048,512]{2,1,0:T(8,128)(2,1)} %up_hbm.1, ...), custom_call_target="tpu_custom_call" | custom-call | tf_op jit(solution)/shard_map/layer/pallas_call | solution.py:449
  121.9 3.5 %fusion.3 = f32[512,512]{0,1:T(8,128)S(1)} fusion(bf16[512,2048]{1,0:T(8,128)(2,1)} %bitcast.47, bf16[2048,128]{1,0:T(8,128)(2,1)} %param.20, bf16[2048,128]{1,0:T(8,128)(2,1)} %param.19, bf16[2048,256]{1,0:T(8,128)(2,1)} %param.18), kind=kOutput, calls=%fused_computation.6 | convolution fusion | flops 1080033280 | bytes 5242880 | tf_op jit(solution)/shard_map/dot_general | solution.py:536
  125.3 0.0 copy-start.3
  125.4 0.3 multiply_cosine_fusion
  125.8 2.9 %collective-permute-start.1 = (bf16[128,256]{0,1:T(8,128)(2,1)S(1)}, bf16[128,256]{0,1:T(8,128)(2,1)S(1)}, u32[]{:S(2)}, u32[]{:S(2)}) collective-permute-start(bf16[128,256]{0,1:T(8,128)(2,1)S(1)} %get-tuple-element.44), channel_id=1, source_target_pairs={{4,0},{8,4},{12,8},{5,1},{9,5},{13,9},{6,2},{10,6},{14,10},{7,3},{... | collective-permute-start | bytes 196616 | tf_op jit(solution)/shard_map/ppermute | solution.py:27
  128.7 2.9 %collective-permute-start = (bf16[128,256]{0,1:T(8,128)(2,1)S(1)}, bf16[128,256]{0,1:T(8,128)(2,1)S(1)}, u32[]{:S(2)}, u32[]{:S(2)}) collective-permute-start(bf16[128,256]{0,1:T(8,128)(2,1)S(1)} %get-tuple-element.43), channel_id=1, source_target_pairs={{0,4},{4,8},{8,12},{1,5},{5,9},{9,13},{2,6},{6,10},{10,14},{3,7},{... | collective-permute-start | bytes 196616 | tf_op jit(solution)/shard_map/ppermute | solution.py:24
  131.7 0.1 subtract_convert_fusion
  131.7 0.8 fusion.10
  132.5 0.0 copy-done.3
  132.5 0.1 max.22
  132.6 0.0 collective-permute-done.1
  132.6 0.1 collective-permute-done
  132.8 1.3 fusion.1
  134.1 0.1 broadcast_maximum_fusion
  134.1 1.4 fusion
  135.5 0.1 exponential_add_fusion
  135.6 0.0 copy-start.2
  135.6 2.0 %fusion.11 = bf16[2,64,2,512]{3,1,2,0:T(8,128)(2,1)S(1)} fusion(bf16[768,2,64,1]{0,2,3,1:T(8,128)(2,1)S(1)} %bitcast.43, f32[2,768,512,2]{2,1,3,0:T(8,128)S(1)} %get-tuple-element.50, f32[2,2,512]{2,1,0:T(2,128)S(1)} %exponential_add_fusion, f32[2,2,512]{2,1,0:T(2,128)S(1)} %broadcast_maximum_fusion, pred[512,768]{0,1:T(8,128)(4,1)S(1)} %fusion.10), kind=kOutput, calls=%fused_computation.19 | convolution fusion | flops 209321984 | bytes 7159808 | tf_op jit(solution)/shard_map/while/body/eval_jaxpr/kgqc,ckd->qkgd/dot_general | solution.py:85
  137.6 0.8 copy.22
  138.5 0.0 copy-done.2
  138.5 0.8 copy.27
  (16 shorter events, 0.3 us)
Async XLA Ops:
  0.6 5.7 %copy-start = (bf16[2048,16]{0,1:T(8,128)(2,1)S(1)}, bf16[2048,16]{0,1:T(8,128)(2,1)}, u32[]{:S(2)}) copy-start(bf16[2048,16]{0,1:T(8,128)(2,1)} %param.24) | copy-start | bytes 196612
  6.3 0.9 copy-start.1
  125.3 7.2 %copy-start.3 = (f32[4]{0:T(128)S(1)}, f32[4]{0:T(128)}, u32[]{:S(2)}) copy-start(f32[4]{0:T(128)} %param.21) | copy-start | bytes 52
  125.8 6.8 %collective-permute-start.1 = (bf16[128,256]{0,1:T(8,128)(2,1)S(1)}, bf16[128,256]{0,1:T(8,128)(2,1)S(1)}, u32[]{:S(2)}, u32[]{:S(2)}) collective-permute-start(bf16[128,256]{0,1:T(8,128)(2,1)S(1)} %get-tuple-element.44), channel_id=1, source_target_pairs={{4,0},{8,4},{12,8},{5,1},{9,5},{13,9},{6,2},{10,6},{14,10},{7,3},{... | collective-permute-start | bytes 196616 | tf_op jit(solution)/shard_map/ppermute | solution.py:27
  128.7 4.0 %collective-permute-start = (bf16[128,256]{0,1:T(8,128)(2,1)S(1)}, bf16[128,256]{0,1:T(8,128)(2,1)S(1)}, u32[]{:S(2)}, u32[]{:S(2)}) collective-permute-start(bf16[128,256]{0,1:T(8,128)(2,1)S(1)} %get-tuple-element.43), channel_id=1, source_target_pairs={{0,4},{4,8},{8,12},{1,5},{5,9},{9,13},{2,6},{6,10},{10,14},{3,7},{... | collective-permute-start | bytes 196616 | tf_op jit(solution)/shard_map/ppermute | solution.py:24
  135.6 2.9 %copy-start.2 = (bf16[128,2048]{1,0:T(8,128)(2,1)S(1)}, bf16[128,2048]{1,0:T(8,128)(2,1)}, u32[]{:S(2)}) copy-start(bf16[128,2048]{1,0:T(8,128)(2,1)} %get-tuple-element.60) | copy-start | bytes 1572868

commit v5 on v4

--- a/solution.py
+++ b/solution.py
@@ -129,9 +129,9 @@
 
 def layer_kernel(
     ep_count, tp_count, slots,
-    second, first, meta, gate_hbm, up_hbm, down_hbm, sgate, sup, sdown,
-    out, gath1,
-    gath2, metag, sbuf, disp, back, sides, psend, gate, up, down, hidden, hexp,
+    second, first, meta, gate_hbm, up_hbm, down_hbm, sgate, sup, sdown, wq, wk, wv,
+    out, query, key, value_rows,
+    gath1, gath2, metag, sbuf, disp, back, sides, psend, gate, up, down, hidden, hexp,
     own_sem, w_sem, s2, r2, sm, rm, s1, r1, sd, rd, sb, rb, sp, rs,
 ):
     grp, ep, tp = lax.axis_index("grp"), lax.axis_index("ep"), lax.axis_index("tp")
@@ -319,6 +319,16 @@
     lax.fori_loop(1, tp_count, hop, 0)
     own_copies[2].wait()
 
+    def project(block):
+        values = gath1[block]
+        query[block] = jnp.dot(values, wq[...], preferred_element_type=jnp.float32)
+        key[block] = jnp.dot(values, wk[...], preferred_element_type=jnp.float32)
+        value_rows[block] = jnp.dot(
+            values, wv[...], preferred_element_type=jnp.float32
+        ).astype(jnp.bfloat16)
+
+    project(tp)
+
     def partial_of(block):
         pieces = []
         for d in range(ep_count):
@@ -389,6 +399,13 @@
 
         reduce_step(2 * k - 1)
         reduce_step(2 * k)
+        for side in range(2):
+            block = tp - k if side == 0 else tp + k
+
+            @pl.when(block >= 0 if side == 0 else block < tp_count)
+            def _():
+                project(block)
+
         return carry
 
     lax.fori_loop(1, tp_count, hop_first, 0)
@@ -439,7 +456,7 @@
     lax.fori_loop(0, tp_count, finish, 0)
 
 
-def layer(second, first, meta, gate, up, down, sgate, sup, sdown, ep_count, tp_count, slots):
+def layer(second, first, meta, gate, up, down, sgate, sup, sdown, wq, wk, wv, ep_count, tp_count, slots):
     rows, width = second.shape
     vmem = pl.BlockSpec(memory_space=pltpu.VMEM)
     hbm = pl.BlockSpec(memory_space=pl.ANY)
@@ -450,11 +467,14 @@
         functools.partial(layer_kernel, ep_count, tp_count, slots),
         out_shape=(
             jax.ShapeDtypeStruct((rows, width), bf16),
-            jax.ShapeDtypeStruct((tp_count, rows, width), bf16),
+            jax.ShapeDtypeStruct((tp_count, rows, wq.shape[1]), jnp.float32),
+            jax.ShapeDtypeStruct((tp_count, rows, wk.shape[1]), jnp.float32),
+            jax.ShapeDtypeStruct((tp_count, rows, wv.shape[1]), bf16),
         ),
-        in_specs=[vmem] * 3 + [hbm] * 3 + [vmem] * 3,
-        out_specs=(vmem, vmem),
+        in_specs=[vmem] * 3 + [hbm] * 3 + [vmem] * 6,
+        out_specs=(vmem,) * 4,
         scratch_shapes=[
+            pltpu.VMEM((tp_count, rows, width), bf16),
             pltpu.VMEM((tp_count, rows, width), bf16),
             pltpu.VMEM((tp_count,) + meta.shape, jnp.float32),
             pltpu.VMEM((tp_count, total, width), bf16),
@@ -486,7 +506,7 @@
             collective_id=0, has_side_effects=True, vmem_limit_bytes=VMEM_LIMIT
         ),
         name="layer",
-    )(second, first, meta, gate, up, down, sgate, sup, sdown)
+    )(second, first, meta, gate, up, down, sgate, sup, sdown, wq, wk, wv)
 
 
 def body(
@@ -526,27 +546,22 @@
     places = jnp.where(hits, before, -1.0)
     meta = jnp.concatenate([places, route_weight], axis=1).T
     width = normed_second.shape[1]
-    moe_out, gathered_first = layer(
+    moe_out, query_part, key_part, value_part = layer(
         normed_second, normed_first, meta, expert_gate, expert_up, expert_down,
-        shared_gate, shared_up, shared_down, ep_count, tp_count, slots,
+        shared_gate, shared_up, shared_down, w_query, w_key, w_value, ep_count, tp_count, slots,
     )
-    query_cols = w_query.shape[1]
     key_cols = w_key.shape[1]
-    joined = jnp.concatenate([w_query, w_key, w_value], axis=1)
-    projected = jnp.dot(
-        gathered_first.reshape(-1, width), joined, preferred_element_type=jnp.float32
-    )
-    span_rows = projected.shape[0]
+    span_rows = tokens * tp_count
     offset = lax.axis_index("ep") * span_rows
     seq_length = span_rows * ep_count
     positions = offset + jnp.arange(span_rows, dtype=jnp.int32)
     query_rows = rotate(
-        projected[:, :query_cols].reshape(span_rows, -1, HEAD_DIM), positions
+        query_part.reshape(span_rows, -1, HEAD_DIM), positions
     ).astype(jnp.bfloat16)
     key_rows = rotate(
-        projected[:, query_cols : query_cols + key_cols].reshape(span_rows, -1, HEAD_DIM), positions
+        key_part.reshape(span_rows, -1, HEAD_DIM), positions
     ).astype(jnp.bfloat16)
-    value_rows = projected[:, query_cols + key_cols :].astype(jnp.bfloat16)
+    value_rows = value_part.reshape(span_rows, -1)
     stacked = jnp.concatenate([key_rows.reshape(span_rows, key_cols), value_rows], axis=1)
     padded = extended(stacked, (("ep", 0),), WINDOW)
     mixed = attend(query_rows, padded, sink_logit, offset, seq_length)

time: 140 us -> 140 us (level)
  local copies, waits for them, and re-layouts: 1.85 us -> 5.46 us
  matrix products: 7.21 us -> 3.75 us
    dot_general x1 -> x0, matrix products: 3.47 us -> none  [body(): jnp.dot(gathered_first.reshape(-1, width), joined, preferred_element_type...]
    pallas_call x0 -> x2, local copies, waits for them, and re-layouts: none -> 2.36 us  [layer(): pl.pallas_call(functools.partial(layer_kernel, ep_count, tp_count, slots)...]
  transfers between devices with their start and end apart: 2 -> 2, of which waited for: 1 -> 0; matrix products, arithmetic and copies ran while one was open for 1% -> 2% of each run, Pallas kernels for 0% -> 0%
where the time goes in v5:
time: 140 us
  Pallas kernels  115 us (82%)
  other arithmetic  8.85 us (6%)
  starting transfers between devices  5.74 us (4%)
  local copies, waits for them, and re-layouts  5.46 us (4%)
  matrix products  3.75 us (3%)
    pallas_call x1, Pallas kernels, layer(): pl.pallas_call(functools.partial(layer_kernel, ep_count, tp_count, slots)...  115 us
    ppermute x1, starting transfers between devices, extended(): lax.ppermute(lax.slice_in_dim(block, block.shape[dim] - width, None, axis...  3.26 us
  transfers between devices with their start and end apart: 2, of which 0 were waited for; matrix products, arithmetic and copies ran while one was open for 2% of the time, Pallas kernels for 0%

profile of v5, /device:TPU:1, one launch (start us, length us, event | category | flops | bytes accessed | tf_op | source)
XLA Modules:
  0.0 140.1 jit_solution(868856072248723483)
XLA Ops:
  0.6 0.0 copy-start
  0.7 1.2 fusion.10
  1.9 1.2 fusion.13
  3.2 0.7 fusion.23
  3.9 0.2 convolution_select_fusion
  4.1 2.2 %fusion.12 = (bf16[128,2048]{1,0:T(8,128)(2,1)S(1)}, bf16[128,2048]{1,0:T(8,128)(2,1)}) fusion(bf16[128,2048]{1,0:T(8,128)(2,1)} %param.22, f32[2048]{0:T(1024)} %param.23, f32[128]{0:T(128)S(1)} %add_rsqrt_fusion.1, f32[2048]{0:T(1024)} %param.17, f32[128]{0:T(128)S(1)} %add_rsqrt_fusion, bf16[128,2048]{1,0:T(8,128)(2,1)} %param.16), kind=kLoop, calls=%fused_computation.22 | loop fusion | flops 2097152 | bytes 2114560 | tf_op jit(solution)/shard_map/convert_element_type | solution.py:35
  6.3 0.0 copy-start.1
  6.3 0.0 copy-done
  6.3 0.3 fusion.35
  6.6 0.6 maximum_bitcast_fusion.meta
  7.2 0.0 copy-done.1
  7.2 0.0 copy-start.3
  7.2 115.4 %layer.1 = (bf16[128,2048]{1,0:T(8,128)(2,1)}, f32[4,128,256]{2,1,0:T(8,128)}, f32[4,128,128]{2,1,0:T(8,128)}, bf16[4,128,128]{2,1,0:T(8,128)(2,1)}) custom-call(bf16[128,2048]{1,0:T(8,128)(2,1)} %copy-done.1, bf16[128,2048]{1,0:T(8,128)(2,1)} %get-tuple-element.58.first, f32[32,128]{1,0:T(8,128)} %maximum_bitcast_fusion.meta, ...), custom_call_target="tpu_custom_call" | custom-call | tf_op jit(solution)/shard_map/layer/pallas_call | solution.py:466
  122.7 1.0 copy.32
  123.7 1.1 copy.31
  124.8 0.1 reshape.204
  124.9 0.3 multiply_cosine_fusion
  125.3 2.5 %collective-permute-start.1 = (bf16[128,256]{0,1:T(8,128)(2,1)S(1)}, bf16[128,256]{0,1:T(8,128)(2,1)S(1)}, u32[]{:S(2)}, u32[]{:S(2)}) collective-permute-start(bf16[128,256]{0,1:T(8,128)(2,1)S(1)} %get-tuple-element.50), channel_id=1, source_target_pairs={{4,0},{8,4},{12,8},{5,1},{9,5},{13,9},{6,2},{10,6},{14,10},{7,3},{... | collective-permute-start | bytes 196616 | tf_op jit(solution)/shard_map/ppermute | solution.py:27
  127.8 3.3 %collective-permute-start = (bf16[128,256]{0,1:T(8,128)(2,1)S(1)}, bf16[128,256]{0,1:T(8,128)(2,1)S(1)}, u32[]{:S(2)}, u32[]{:S(2)}) collective-permute-start(bf16[128,256]{0,1:T(8,128)(2,1)S(1)} %get-tuple-element.49), channel_id=1, source_target_pairs={{0,4},{4,8},{8,12},{1,5},{5,9},{9,13},{2,6},{6,10},{10,14},{3,7},{... | collective-permute-start | bytes 196616 | tf_op jit(solution)/shard_map/ppermute | solution.py:24
  131.1 1.3 copy.33
  132.4 0.2 reshape.208
  132.6 0.1 subtract_convert_fusion
  132.7 0.8 fusion.4
  133.5 0.0 copy-done.3
  133.5 0.1 max.22
  133.5 0.0 collective-permute-done.1
  133.5 0.0 collective-permute-done
  133.6 1.3 fusion.1
  134.9 0.1 broadcast_maximum_fusion
  135.0 1.4 fusion
  136.3 0.1 exponential_add_fusion
  136.4 0.0 copy-start.2
  136.4 2.0 %fusion.5 = bf16[2,64,2,512]{3,1,2,0:T(8,128)(2,1)S(1)} fusion(bf16[768,2,64,1]{0,2,3,1:T(8,128)(2,1)S(1)} %bitcast.42, f32[2,768,512,2]{2,1,3,0:T(8,128)S(1)} %get-tuple-element.56, f32[2,2,512]{2,1,0:T(2,128)S(1)} %exponential_add_fusion, f32[2,2,512]{2,1,0:T(2,128)S(1)} %broadcast_maximum_fusion, pred[512,768]{0,1:T(8,128)(4,1)S(1)} %fusion.4), kind=kOutput, calls=%fused_computation.13 | convolution fusion | flops 209321984 | bytes 7159808 | tf_op jit(solution)/shard_map/while/body/eval_jaxpr/kgqc,ckd->qkgd/dot_general | solution.py:85
  138.4 0.8 copy.35
  139.3 0.0 copy-done.2
  139.3 0.8 copy.40
  (13 shorter events, 0.2 us)
Async XLA Ops:
  0.6 5.7 %copy-start = (bf16[2048,16]{0,1:T(8,128)(2,1)S(1)}, bf16[2048,16]{0,1:T(8,128)(2,1)}, u32[]{:S(2)}) copy-start(bf16[2048,16]{0,1:T(8,128)(2,1)} %param.24) | copy-start | bytes 196612
  6.3 0.9 copy-start.1
  7.2 126.2 %copy-start.3 = (f32[4]{0:T(128)S(1)}, f32[4]{0:T(128)}, u32[]{:S(2)}) copy-start(f32[4]{0:T(128)} %param.21) | copy-start | bytes 52
  125.3 8.2 %collective-permute-start.1 = (bf16[128,256]{0,1:T(8,128)(2,1)S(1)}, bf16[128,256]{0,1:T(8,128)(2,1)S(1)}, u32[]{:S(2)}, u32[]{:S(2)}) collective-permute-start(bf16[128,256]{0,1:T(8,128)(2,1)S(1)} %get-tuple-element.50), channel_id=1, source_target_pairs={{4,0},{8,4},{12,8},{5,1},{9,5},{13,9},{6,2},{10,6},{14,10},{7,3},{... | collective-permute-start | bytes 196616 | tf_op jit(solution)/shard_map/ppermute | solution.py:27
  127.8 5.8 %collective-permute-start = (bf16[128,256]{0,1:T(8,128)(2,1)S(1)}, bf16[128,256]{0,1:T(8,128)(2,1)S(1)}, u32[]{:S(2)}, u32[]{:S(2)}) collective-permute-start(bf16[128,256]{0,1:T(8,128)(2,1)S(1)} %get-tuple-element.49), channel_id=1, source_target_pairs={{0,4},{4,8},{8,12},{1,5},{5,9},{9,13},{2,6},{6,10},{10,14},{3,7},{... | collective-permute-start | bytes 196616 | tf_op jit(solution)/shard_map/ppermute | solution.py:24
  136.4 2.9 %copy-start.2 = (bf16[128,2048]{1,0:T(8,128)(2,1)S(1)}, bf16[128,2048]{1,0:T(8,128)(2,1)}, u32[]{:S(2)}) copy-start(bf16[128,2048]{1,0:T(8,128)(2,1)} %get-tuple-element.66) | copy-start | bytes 1572868

commit v6 on v5

--- a/solution.py
+++ b/solution.py
@@ -35,21 +35,17 @@
     return (values * factor * gain_vector).astype(jnp.bfloat16)
 
 
-def rotate(head_rows, positions):
-    half_width = head_rows.shape[-1] // 2
-    inverse = THETA ** (-(jnp.arange(half_width, dtype=jnp.float32) * 2.0) / head_rows.shape[-1])
+def rotate(flat_rows, positions):
+    half_width = HEAD_DIM // 2
+    channel = jnp.arange(flat_rows.shape[-1], dtype=jnp.int32) % HEAD_DIM
+    place = (channel % half_width).astype(jnp.float32)
+    inverse = THETA ** (-(place * 2.0) / HEAD_DIM)
     angles = positions.astype(jnp.float32)[:, None] * inverse[None, :]
-    cosine_table = jnp.cos(angles)[:, None, :]
-    sine_table = jnp.sin(angles)[:, None, :]
-    first_half = head_rows[..., :half_width]
-    second_half = head_rows[..., half_width:]
-    return jnp.concatenate(
-        [
-            first_half * cosine_table - second_half * sine_table,
-            second_half * cosine_table + first_half * sine_table,
-        ],
-        axis=-1,
+    lower = (channel < half_width)[None, :]
+    partner = jnp.where(
+        lower, jnp.roll(flat_rows, -half_width, axis=1), jnp.roll(flat_rows, half_width, axis=1)
     )
+    return flat_rows * jnp.cos(angles) + partner * jnp.where(lower, -jnp.sin(angles), jnp.sin(angles))
 
 
 def attend(query_rows, stacked, sink_logit, offset, seq_length):
@@ -327,7 +323,6 @@
             values, wv[...], preferred_element_type=jnp.float32
         ).astype(jnp.bfloat16)
 
-    project(tp)
 
     def partial_of(block):
         pieces = []
@@ -409,6 +404,7 @@
         return carry
 
     lax.fori_loop(1, tp_count, hop_first, 0)
+    project(tp)
     wait_return(tp)
     own_value = partial_of(tp)
 
@@ -550,19 +546,15 @@
         normed_second, normed_first, meta, expert_gate, expert_up, expert_down,
         shared_gate, shared_up, shared_down, w_query, w_key, w_value, ep_count, tp_count, slots,
     )
-    key_cols = w_key.shape[1]
     span_rows = tokens * tp_count
     offset = lax.axis_index("ep") * span_rows
     seq_length = span_rows * ep_count
     positions = offset + jnp.arange(span_rows, dtype=jnp.int32)
-    query_rows = rotate(
-        query_part.reshape(span_rows, -1, HEAD_DIM), positions
-    ).astype(jnp.bfloat16)
-    key_rows = rotate(
-        key_part.reshape(span_rows, -1, HEAD_DIM), positions
-    ).astype(jnp.bfloat16)
+    query_rows = rotate(query_part.reshape(span_rows, -1), positions).astype(jnp.bfloat16)
+    query_rows = query_rows.reshape(span_rows, -1, HEAD_DIM)
+    key_rows = rotate(key_part.reshape(span_rows, -1), positions).astype(jnp.bfloat16)
     value_rows = value_part.reshape(span_rows, -1)
-    stacked = jnp.concatenate([key_rows.reshape(span_rows, key_cols), value_rows], axis=1)
+    stacked = jnp.concatenate([key_rows, value_rows], axis=1)
     padded = extended(stacked, (("ep", 0),), WINDOW)
     mixed = attend(query_rows, padded, sink_logit, offset, seq_length)
     return (mixed, moe_out)

time: 140 us -> 148 us (1.057)
  other arithmetic: 8.85 us -> 11.8 us
  local copies, waits for them, and re-layouts: 5.46 us -> 7.68 us
  matrix products: 3.75 us -> 5.75 us
    slice x0 -> x5, local copies, waits for them, and re-layouts: none -> 3.87 us  [the longest x4 3.73 us: rotate(): jnp.roll(flat_rows, half_width, axis=1)]
    convert_element_type x0 -> x1, other arithmetic: none -> 2.17 us  [body(): rotate(key_part.reshape(span_rows, -1), positions).astype(jnp.bfloat16)]
    dot_general x1, matrix products: 1.27 us -> 3.28 us  [one_block(): jnp.einsum('qkgd,ckd->kgqc', query_block, key_block, preferred_element_ty...]
  transfers between devices with their start and end apart: 2 -> 2, of which waited for: 0 -> 0; matrix products, arithmetic and copies ran while one was open for 2% -> 3% of each run, Pallas kernels for 0% -> 0%
where the time goes in v6:
time: 148 us; the launch traced here: 147 us
  Pallas kernels  115 us (78%)
  other arithmetic  11.8 us (8%)
  local copies, waits for them, and re-layouts  7.68 us (5%)
  matrix products  5.75 us (4%)
  starting transfers between devices  5.74 us (4%)
    pallas_call x1, Pallas kernels, layer(): pl.pallas_call(functools.partial(layer_kernel, ep_count, tp_count, slots)...  115 us
    slice x4, local copies, waits for them, and re-layouts, rotate(): jnp.roll(flat_rows, half_width, axis=1)  3.73 us
    dot_general x1, matrix products, one_block(): jnp.einsum('qkgd,ckd->kgqc', query_block, key_block, preferred_element_ty...  3.28 us
  transfers between devices with their start and end apart: 2, of which 0 were waited for; matrix products, arithmetic and copies ran while one was open for 3% of the time, Pallas kernels for 0%

profile of v6, /device:TPU:1, one launch (start us, length us, event | category | flops | bytes accessed | tf_op | source)
XLA Modules:
  0.0 147.2 jit_solution(8207726483369129578)
XLA Ops:
  0.6 0.0 copy-start
  0.7 1.3 fusion.10
  1.9 1.2 fusion.13
  3.2 0.7 fusion.32
  3.9 0.2 convolution_select_fusion
  4.1 2.2 %fusion.12 = (bf16[128,2048]{1,0:T(8,128)(2,1)S(1)}, bf16[128,2048]{1,0:T(8,128)(2,1)}) fusion(bf16[128,2048]{1,0:T(8,128)(2,1)} %param.22, f32[2048]{0:T(1024)} %param.23, f32[128]{0:T(128)S(1)} %add_rsqrt_fusion.1, f32[2048]{0:T(1024)} %param.17, f32[128]{0:T(128)S(1)} %add_rsqrt_fusion, bf16[128,2048]{1,0:T(8,128)(2,1)} %param.16), kind=kLoop, calls=%fused_computation.22 | loop fusion | flops 2097152 | bytes 2114560 | tf_op jit(solution)/shard_map/convert_element_type | solution.py:35
  6.3 0.0 copy-start.2
  6.3 0.0 copy-done
  6.3 0.3 fusion.59
  6.6 0.6 maximum_bitcast_fusion.meta
  7.2 0.0 copy-done.2
  7.2 115.4 %layer.1 = (bf16[128,2048]{1,0:T(8,128)(2,1)}, f32[4,128,256]{2,1,0:T(8,128)}, f32[4,128,128]{2,1,0:T(8,128)}, bf16[4,128,128]{2,1,0:T(8,128)(2,1)}) custom-call(bf16[128,2048]{1,0:T(8,128)(2,1)} %copy-done.2, bf16[128,2048]{1,0:T(8,128)(2,1)} %get-tuple-element.60.first, f32[32,128]{1,0:T(8,128)} %maximum_bitcast_fusion.meta, ...), custom_call_target="tpu_custom_call" | custom-call | tf_op jit(solution)/shard_map/layer/pallas_call | solution.py:462
  122.6 0.0 copy-start.1
  122.6 1.2 fusion.57
  123.8 0.0 copy-start.5
  123.8 1.2 fusion.58
  125.0 0.0 copy-start.4
  125.1 2.2 %fusion.22 = bf16[512,128]{1,0:T(8,128)(2,1)S(1)} fusion(f32[512,32]{1,0:T(8,128)S(1)} %get-tuple-element.52, f32[512,96]{1,0:T(8,128)S(1)} %get-tuple-element.54, f32[512,96]{1,0:T(8,128)S(1)} %get-tuple-element.53, f32[512,32]{1,0:T(8,128)S(1)} %get-tuple-element.51, f32[128]{0:T(128)S(1)} %fusion.48, f32[512]{0:T(512)S(1)} %get-tuple-element.62, ...), kind=kLoop, calls=%fused_computation.41 | loop fusion | flops 655360 | bytes 920192 | tf_op jit(solution)/shard_map/convert_element_type | solution.py:555
  127.2 0.8 pad_maximum_fusion.4
  128.0 2.9 %collective-permute-start.1 = (bf16[128,256]{1,0:T(8,128)(2,1)S(1)}, bf16[128,256]{1,0:T(8,128)(2,1)S(1)}, u32[]{:S(2)}, u32[]{:S(2)}) collective-permute-start(bf16[128,256]{1,0:T(8,128)(2,1)S(1)} %get-tuple-element.50), channel_id=1, source_target_pairs={{4,0},{8,4},{12,8},{5,1},{9,5},{13,9},{6,2},{10,6},{14,10},{7,3},{... | collective-permute-start | bytes 196616 | tf_op jit(solution)/shard_map/ppermute | solution.py:27
  130.9 2.9 %collective-permute-start = (bf16[128,256]{1,0:T(8,128)(2,1)S(1)}, bf16[128,256]{1,0:T(8,128)(2,1)S(1)}, u32[]{:S(2)}, u32[]{:S(2)}) collective-permute-start(bf16[128,256]{1,0:T(8,128)(2,1)S(1)} %get-tuple-element.49), channel_id=1, source_target_pairs={{0,4},{4,8},{8,12},{1,5},{5,9},{9,13},{2,6},{6,10},{10,14},{3,7},{... | collective-permute-start | bytes 196616 | tf_op jit(solution)/shard_map/ppermute | solution.py:24
  133.8 1.3 copy.36
  135.1 1.2 fusion.54
  136.3 0.0 copy-done.1
  136.3 0.2 fusion.55
  136.5 0.2 reshape.227
  136.7 0.1 pad_maximum_fusion
  136.9 0.2 copy.37
  137.1 0.2 pad_maximum_fusion.1
  137.3 0.2 copy.38
  137.5 0.0 copy-done.5
  137.5 0.1 max.22
  137.6 0.7 fusion.4
  138.3 0.0 collective-permute-done.1
  138.3 0.0 collective-permute-done
  138.4 0.0 copy-done.4
  138.5 0.1 copy.34
  138.6 0.1 copy.35
  138.8 3.3 %fusion.1 = (f32[2,2,512]{2,1,0:T(2,128)S(1)}, f32[2,768,512,2]{2,1,3,0:T(8,128)S(1)}) fusion(pred[512,768]{0,1:T(8,128)(4,1)S(1)} %fusion.4, bf16[768,2,64,1]{0,2,3,1:T(8,128)(2,1)S(1)} %bitcast.49, f32[512,2,2,64]{0,3,2,1:T(8,128)S(1)} %reshape.227, f32[512,2,2,64]{0,3,2,1:T(8,128)S(1)} %bitcast.43, f32[512,2,2,64]{0,3,2,1:T(8,128)S(1)} %bitcast.44, ...), kind=kOutput, calls=%fused_computation.4 | convolution fusion | flops 207091712 | bytes 8465664 | tf_op jit(solution)/shard_map/while/body/eval_jaxpr/qkgd,ckd->kgqc/dot_general | solution.py:68
  142.0 0.1 broadcast_maximum_fusion
  142.1 1.4 fusion
  143.5 0.1 exponential_add_fusion
  143.6 0.0 copy-start.3
  143.6 2.0 %fusion.5 = bf16[2,64,2,512]{3,1,2,0:T(8,128)(2,1)S(1)} fusion(bf16[768,2,64,1]{0,2,3,1:T(8,128)(2,1)S(1)} %bitcast.48, f32[2,768,512,2]{2,1,3,0:T(8,128)S(1)} %get-tuple-element.58, f32[2,2,512]{2,1,0:T(2,128)S(1)} %exponential_add_fusion, f32[2,2,512]{2,1,0:T(2,128)S(1)} %broadcast_maximum_fusion, pred[512,768]{0,1:T(8,128)(4,1)S(1)} %fusion.4), kind=kOutput, calls=%fused_computation.13 | convolution fusion | flops 209321984 | bytes 7159808 | tf_op jit(solution)/shard_map/while/body/eval_jaxpr/kgqc,ckd->qkgd/dot_general | solution.py:81
  145.6 0.8 copy.40
  146.4 0.0 copy-done.3
  146.4 0.8 copy.45
  (13 shorter events, 0.2 us)
Async XLA Ops:
  0.6 5.7 %copy-start = (bf16[2048,16]{0,1:T(8,128)(2,1)S(1)}, bf16[2048,16]{0,1:T(8,128)(2,1)}, u32[]{:S(2)}) copy-start(bf16[2048,16]{0,1:T(8,128)(2,1)} %param.24) | copy-start | bytes 196612
  6.3 0.9 copy-start.2
  122.6 13.7 %copy-start.1 = (f32[4,128,256]{2,1,0:T(8,128)S(1)}, f32[4,128,256]{2,1,0:T(8,128)}, u32[]{:S(2)}) copy-start(f32[4,128,256]{2,1,0:T(8,128)} %get-tuple-element.26) | copy-start | bytes 1572868
  123.8 13.7 %copy-start.5 = (f32[4]{0:T(128)S(1)}, f32[4]{0:T(128)}, u32[]{:S(2)}) copy-start(f32[4]{0:T(128)} %param.21) | copy-start | bytes 52
  125.0 13.4 %copy-start.4 = (bf16[4,128,128]{2,1,0:T(8,128)(2,1)S(1)}, bf16[4,128,128]{2,1,0:T(8,128)(2,1)}, u32[]{:S(2)}) copy-start(bf16[4,128,128]{2,1,0:T(8,128)(2,1)} %get-tuple-element.25) | copy-start | bytes 393220
  128.0 10.3 %collective-permute-start.1 = (bf16[128,256]{1,0:T(8,128)(2,1)S(1)}, bf16[128,256]{1,0:T(8,128)(2,1)S(1)}, u32[]{:S(2)}, u32[]{:S(2)}) collective-permute-start(bf16[128,256]{1,0:T(8,128)(2,1)S(1)} %get-tuple-element.50), channel_id=1, source_target_pairs={{4,0},{8,4},{12,8},{5,1},{9,5},{13,9},{6,2},{10,6},{14,10},{7,3},{... | collective-permute-start | bytes 196616 | tf_op jit(solution)/shard_map/ppermute | solution.py:27
  130.9 7.4 %collective-permute-start = (bf16[128,256]{1,0:T(8,128)(2,1)S(1)}, bf16[128,256]{1,0:T(8,128)(2,1)S(1)}, u32[]{:S(2)}, u32[]{:S(2)}) collective-permute-start(bf16[128,256]{1,0:T(8,128)(2,1)S(1)} %get-tuple-element.49), channel_id=1, source_target_pairs={{0,4},{4,8},{8,12},{1,5},{5,9},{9,13},{2,6},{6,10},{10,14},{3,7},{... | collective-permute-start | bytes 196616 | tf_op jit(solution)/shard_map/ppermute | solution.py:24
  143.6 2.9 %copy-start.3 = (bf16[128,2048]{1,0:T(8,128)(2,1)S(1)}, bf16[128,2048]{1,0:T(8,128)(2,1)}, u32[]{:S(2)}) copy-start(bf16[128,2048]{1,0:T(8,128)(2,1)} %get-tuple-element.68) | copy-start | bytes 1572868
